TPU v7x, 512 devices: a whole 4x8x8 slice. The times are simulated.
512 devices in a mesh: kv: 64 (over z, y), tp: 8 (over x, core).
Axes of the slice: x: 4, y: 8, z: 8, core: 2. Of those that a mesh axis runs over, the one named last changes fastest.
Arguments:
- tokens: bfloat16 [16, 4096], P(None, 'kv'), may hold values from -32 to 32
- attn_gain: float32 [4096], P('kv'), may hold values from 0.1 to 1.9
- w_query: bfloat16 [4096, 4096], P('kv', 'tp'), may hold values from -0.09375 to 0.09375
- w_key: bfloat16 [4096, 4096], P('kv', 'tp'), may hold values from -0.09375 to 0.09375
- w_value: bfloat16 [4096, 4096], P('kv', 'tp'), may hold values from -0.09375 to 0.09375
- key_cache: bfloat16 [16, 8192, 32, 128], P(None, 'kv', 'tp'), may hold values from -128 to 128
- value_cache: bfloat16 [16, 8192, 32, 128], P(None, 'kv', 'tp'), may hold values from -6 to 6
- lengths: int32 [16], replicated, may hold values from 1 to 8192, as said below
- mix_weight: float32 [32], P('tp'), may hold values from 0.3 to 0.8
- head_gain: float32 [128], replicated, may hold values from 0.1 to 1.9
- w_out: bfloat16 [4096, 4096], P('tp', 'kv'), may hold values from -0.09375 to 0.09375
- mixer_gain: float32 [4096], P('kv'), may hold values from 0.1 to 1.9
- w_gate: bfloat16 [4096, 11264], P('kv', 'tp'), may hold values from -0.09375 to 0.09375
- w_up: bfloat16 [4096, 11264], P('kv', 'tp'), may hold values from -0.09375 to 0.09375
- w_down: bfloat16 [11264, 4096], P('tp', 'kv'), may hold values from -0.0546875 to 0.0546875
Outputs:
- layer_out: bfloat16 [16, 4096], P(None, 'kv')
Inputs may be any that keep to these rules, and one draw needn't show every extreme that they name: `lengths`: one sequence has exactly 8192 live positions; four or more sequences, a quarter of them or more, have 4 or fewer.
All inputs are finite; a program needn't handle non-finite values.
Results may differ from a plain program's by a relative error of at most 0.017.
Values may be sent and summed in bfloat16 or wider, within the bound.
No kernel may reach another device: no remote copies, remote signals or barrier semaphores. Data moves between devices by JAX's collectives and lax.ppermute only.
A program may use at most 64 MiB of HBM per device.

v0:
```python
import jax
import jax.numpy as jnp
from jax import lax
from jax.sharding import Mesh
from jax.sharding import PartitionSpec as P

KV = ("kv_0", "kv_1")


EPS = 1e-06
FLOOR_SCORE = -1e30


def cut_along(array, dim, devices):
    before, after = (array.shape[:dim], array.shape[dim + 1 :])
    return jnp.moveaxis(array.reshape(*before, devices, -1, *after), dim, 0)


def summed_on_arrival(array, axis, dim):
    devices = lax.axis_size(axis)
    tiles = lax.all_to_all(cut_along(array, dim, devices), axis, 0, 0, tiled=True)
    return jnp.sum(tiles, axis=0)


def rows_for(lines, devices):
    spare = -len(lines) % devices
    return jnp.pad(lines, [(0, spare)] + [(0, 0)] * (lines.ndim - 1))


def from_everyone(array, axis):
    devices = lax.axis_size(axis)
    return lax.all_to_all(
        jnp.broadcast_to(array[None], (devices, *array.shape)), axis, 0, 0, tiled=True
    )


def laid_out(tiles, dim):
    shape = list(tiles.shape[1:])
    shape[dim] *= tiles.shape[0]
    return jnp.moveaxis(tiles, 0, dim).reshape(shape)


def gathered_copies(array, axis, dim):
    tiles = from_everyone(array, axis)
    return laid_out(tiles, dim)


def total_of(array, axes):
    own = summed_on_arrival(rows_for(array, lax.axis_size(axes)), axes, 0)
    whole = gathered_copies(own, axes, 0)
    return whole[: len(array)].reshape(array.shape)


def in_one(arrays, axis):
    ends = [0]
    for a in arrays:
        ends.append(ends[-1] + a.size)
    so_far = total_of(jnp.concatenate([a.ravel() for a in arrays]), axis)
    return tuple((so_far[b:e].reshape(a.shape) for a, b, e in zip(arrays, ends, ends[1:])))


def all_in_one(array, axis):
    leaves = jax.tree.leaves(array)
    sequence = sorted(range(len(leaves)), key=lambda k: -leaves[k].size)
    width = (1, *leaves[sequence[0]].shape)[-1]
    lines = [
        jnp.pad(leaves[k].reshape(-1), (0, -leaves[k].size % width)).reshape(-1, width)
        for k in sequence
    ]
    both, at, found = (lax.all_gather(jnp.concatenate(lines), axis), 0, {})
    for k, line in zip(sequence, lines):
        share = both[:, at : at + len(line)].reshape(len(both), -1)
        found[k] = share[:, : leaves[k].size].reshape(-1, *leaves[k].shape)
        at += len(line)
    numbers = iter(range(len(leaves)))
    return jax.tree.map(lambda _: found[next(numbers)], array)


def joined_all(array, axes, combine):
    for axis in axes:
        pieces = all_in_one(
            jax.tree.map(
                lambda part, kind: part.astype(kind),
                array,
                (jnp.bfloat16, jnp.bfloat16, jnp.bfloat16),
            ),
            axis,
        )
        widened = [
            jax.tree.map(lambda part, own: part[k].astype(own.dtype), pieces, array)
            for k in range(lax.axis_size(axis))
        ]
        array = widened[0]
        for received in widened[1:]:
            array = combine(array, received)
    return array


def over_copies(array, axis):
    everything = from_everyone(array, axis)
    return jnp.sum(everything.astype(jnp.float32), axis=0)


def combine_parts(first_part, second_part):
    peak_first, totals_first, values_first = first_part
    peak_second, totals_second, values_second = second_part
    peak_score = jnp.maximum(peak_first, peak_second)
    rescale_first = jnp.exp(peak_first - peak_score)
    rescale_second = jnp.exp(peak_second - peak_score)
    return (
        peak_score,
        totals_first * rescale_first + totals_second * rescale_second,
        values_first * rescale_first[..., None] + values_second * rescale_second[..., None],
    )


def local(
    tokens,
    attn_gain,
    w_query,
    w_key,
    w_value,
    key_cache,
    value_cache,
    lengths,
    mix_weight,
    head_gain,
    w_out,
    mixer_gain,
    w_gate,
    w_up,
    w_down,
):
    seq_count = tokens.shape[0]
    head_count = mix_weight.shape[0]
    span_len = key_cache.shape[1]
    head_dim = key_cache.shape[3] // 2
    value_dim = value_cache.shape[3]
    model_width = tokens.shape[1] * lax.axis_size(KV)
    tokens_float = tokens.astype(jnp.float32)
    scaled = (tokens_float * attn_gain).astype(jnp.bfloat16)
    squares, query_sum, key_sum, value_sum = in_one(
        (
            jnp.sum(tokens_float * tokens_float, axis=1),
            jnp.dot(scaled, w_query, preferred_element_type=jnp.float32),
            jnp.dot(scaled, w_key, preferred_element_type=jnp.float32),
            jnp.dot(scaled, w_value, preferred_element_type=jnp.float32),
        ),
        KV,
    )
    inverse = lax.rsqrt(squares / model_width + EPS)[:, None]
    queries = (inverse * query_sum).astype(jnp.bfloat16).reshape(seq_count, head_count, 2, head_dim)
    key_new = (inverse * key_sum).astype(jnp.bfloat16).reshape(seq_count, head_count, 2, head_dim)
    value_new = (inverse * value_sum).astype(jnp.bfloat16).reshape(seq_count, head_count, value_dim)
    logit_scale = head_dim ** (-0.5)
    cached_keys = key_cache.reshape(seq_count, span_len, head_count, 2, head_dim)
    score_matrix = (
        jnp.einsum("bhmd,bphmd->bhmp", queries, cached_keys, preferred_element_type=jnp.float32)
        * logit_scale
    )
    own_score = (
        jnp.sum(queries.astype(jnp.float32) * key_new.astype(jnp.float32), axis=3) * logit_scale
    )
    positions = lax.axis_index(KV) * span_len + jnp.arange(span_len, dtype=jnp.int32)
    visible = (positions[None, :] < lengths[:, None])[:, None, None, :]
    local_peak = jnp.max(jnp.where(visible, score_matrix, FLOOR_SCORE), axis=3)
    weights = jnp.where(visible, jnp.exp(score_matrix - local_peak[..., None]), 0.0)
    local_values = jnp.einsum(
        "bhmp,bphv->bhmv",
        weights.astype(jnp.bfloat16),
        value_cache,
        preferred_element_type=jnp.float32,
    )
    peak_score, totals, accumulated = joined_all(
        (local_peak, jnp.sum(weights, axis=3), local_values), KV, combine_parts
    )
    final_peak = jnp.maximum(peak_score, own_score)
    rescale = jnp.exp(peak_score - final_peak)
    own_weight = jnp.exp(own_score - final_peak)
    own_rounded = lax.optimization_barrier(own_weight.astype(jnp.bfloat16)).astype(jnp.float32)
    totals = totals * rescale + own_weight
    accumulated = (
        accumulated * rescale[..., None]
        + own_rounded[..., None] * value_new.astype(jnp.float32)[:, :, None, :]
    )
    mixture = (
        accumulated[:, :, 0] / totals[:, :, 0, None]
        - mix_weight[None, :, None] * accumulated[:, :, 1] / totals[:, :, 1, None]
    )
    head_scale = lax.rsqrt(jnp.mean(mixture * mixture, axis=2, keepdims=True) + EPS)
    attended = (mixture * head_scale * head_gain).astype(jnp.bfloat16)
    attended = attended.reshape(seq_count, head_count * value_dim)
    attention_contribution = over_copies(
        jnp.dot(attended, w_out, preferred_element_type=jnp.float32).astype(jnp.bfloat16), "tp"
    ).astype(jnp.float32)
    residual = (tokens_float + attention_contribution).astype(jnp.bfloat16)
    residual_f = residual.astype(jnp.float32)
    scaled_mix = (residual_f * mixer_gain).astype(jnp.bfloat16)
    squares_mix = jnp.sum(residual_f * residual_f, axis=1)
    gate_part = jnp.dot(scaled_mix, w_gate, preferred_element_type=jnp.float32)
    up_part = jnp.dot(scaled_mix, w_up, preferred_element_type=jnp.float32)
    squares_all, gate_sum, up_sum = in_one((squares_mix, gate_part, up_part), KV)
    reciprocal_mixture = lax.rsqrt(squares_all / model_width + EPS)[:, None]
    hidden = (jax.nn.silu(reciprocal_mixture * gate_sum) * (reciprocal_mixture * up_sum)).astype(
        jnp.bfloat16
    )
    down_part = jnp.dot(hidden, w_down, preferred_element_type=jnp.float32)
    mixer_term = over_copies(down_part.astype(jnp.bfloat16), "tp").astype(jnp.float32)
    return (residual_f + mixer_term).astype(jnp.bfloat16)


def solution(mesh):
    finer = Mesh(mesh.devices.reshape(8, 8, mesh.shape["tp"]), ("kv_0", "kv_1", "tp"))
    return jax.shard_map(
        local,
        mesh=finer,
        in_specs=(
            P(None, KV),
            P(KV),
            P(KV, "tp"),
            P(KV, "tp"),
            P(KV, "tp"),
            P(None, KV, "tp", None),
            P(None, KV, "tp", None),
            P(),
            P("tp"),
            P(),
            P("tp", KV),
            P(KV),
            P(KV, "tp"),
            P(KV, "tp"),
            P("tp", KV),
        ),
        out_specs=P(None, KV),
        check_vma=False,
    )
```

profile of v0, /device:TPU:1, one launch (start us, length us, event | category | flops | bytes accessed | tf_op | source)
XLA Modules:
  0.0 173.6 jit_solution(13912428024905029504)
XLA Ops:
  0.0 0.9 fusion.46
  1.0 1.0 convolution_bitcast_fusion.2
  2.0 1.0 convolution_bitcast_fusion.1
  3.0 1.0 convolution_bitcast_fusion
  4.1 0.9 all_to_all.26
  5.1 17.1 %all-to-all-start = ((f32[64,1,385]{2,1,0:T(1,128)}), f32[64,1,385]{2,1,0:T(1,128)S(1)}, u32[]{:S(2)}, u32[]{:S(2)}) async-start(f32[64,1,385]{2,1,0:T(1,128)} %all_to_all.26), calls=%async_computation | async-start | bytes 262144 | tf_op jit(solution)/shard_map/all_to_all | solution.py:21
  22.2 4.2 %copy.176 = bf16[16,128,4,128]{1,3,2,0:T(8,128)(2,1)} copy(bf16[16,128,4,128]{3,2,1,0:T(4,128)(2,1)} %param.20) | data formatting | bytes 4194304 | tf_op args[5]
  26.5 7.3 %all-to-all-done = f32[64,1,385]{2,1,0:T(1,128)S(1)} async-done(((f32[64,1,385]{2,1,0:T(1,128)}), f32[64,1,385]{2,1,0:T(1,128)S(1)}, u32[]{:S(2)}, u32[]{:S(2)}) %all-to-all-start) | async-done | bytes 98592 | tf_op jit(solution)/shard_map/all_to_all | solution.py:21
  33.8 0.7 broadcast_in_dim.27
  34.6 4.9 %all-to-all-start.1 = ((f32[64,1,385]{2,1,0:T(1,128)}), f32[64,1,385]{2,1,0:T(1,128)S(1)}, u32[]{:S(2)}, u32[]{:S(2)}) async-start(f32[64,1,385]{2,1,0:T(1,128)} %broadcast_in_dim.27), calls=%async_computation.1 | async-start | bytes 262144 | tf_op jit(solution)/shard_map/all_to_all | solution.py:32
  39.6 11.5 %all-to-all-done.1 = f32[64,1,385]{2,1,0:T(1,128)S(1)} async-done(((f32[64,1,385]{2,1,0:T(1,128)}), f32[64,1,385]{2,1,0:T(1,128)S(1)}, u32[]{:S(2)}, u32[]{:S(2)}) %all-to-all-start.1) | async-done | bytes 98592 | tf_op jit(solution)/shard_map/all_to_all | solution.py:32
  51.0 0.3 reduce.2
  51.3 0.2 reshape.1347
  51.8 0.2 multiply_reduce_fusion
  52.1 2.2 %fusion.34 = f32[16,4,2,1,128]{4,3,2,1,0:T(1,128)S(1)} fusion(bf16[16,128,4,2,64]{1,4,3,2,0:T(8,128)(2,1)} %bitcast.428, bf16[16,4,2,64,1]{3,2,1,0,4:T(2,128)(2,1)S(1)} %bitcast.457), kind=kOutput, calls=%fused_computation.54 | convolution fusion | flops 2097152 | bytes 2179072 | tf_op jit(solution)/shard_map/bhmd,bphmd->bhmp/dot_general | solution.py:158
  54.3 0.2 select_reduce_fusion
  54.5 0.3 fusion.131
  54.8 0.7 fusion.2
  55.9 18.8 %all-gather.2 = bf16[8,130,128]{2,1,0:T(8,128)(2,1)S(1)} all-gather(bf16[1,130,128]{2,1,0:T(8,128)(2,1)S(1)} %maximum_bitcast_fusion), channel_id=2, replica_groups=mesh['kv_0'=8,'kv_1'=8,'tp'=8] {'kv_0'}, dimensions={0}, use_global_device_ids=true | all-gather | bytes 299520 | tf_op jit(solution)/shard_map/all_gather | solution.py:70
  74.7 0.3 fusion.21
  75.1 18.6 %all-gather.3 = bf16[8,130,128]{2,1,0:T(8,128)(2,1)S(1)} all-gather(bf16[1,130,128]{2,1,0:T(8,128)(2,1)S(1)} %maximum_bitcast_fusion.1), channel_id=3, replica_groups=mesh['kv_0'=8,'kv_1'=8,'tp'=8] {'kv_1'}, dimensions={0}, use_global_device_ids=true | all-gather | bytes 299520 | tf_op jit(solution)/shard_map/all_gather | solution.py:70
  94.0 0.2 reshape.1406
  94.2 0.2 reshape.1412
  94.5 0.2 reshape.1411
  94.8 0.2 reshape.1410
  95.1 0.2 reshape.1409
  95.4 0.2 reshape.1408
  95.6 0.2 reshape.1407
  95.9 0.2 reshape.1404
  96.2 0.2 reshape.1402
  96.5 0.2 reshape.1400
  96.7 0.2 reshape.1398
  97.0 0.2 reshape.1396
  97.3 0.2 reshape.1394
  97.6 0.2 reshape.1392
  97.8 0.2 reshape.1391
  98.1 0.2 reshape.1413
  100.4 1.3 fusion.7
  101.8 0.2 fusion.43
  102.5 24.4 %all_to_all.40 = bf16[8,2,512]{2,1,0:T(2,128)(2,1)S(1)} all-to-all(bf16[8,2,512]{2,1,0:T(2,128)(2,1)S(1)} %reshape.1513), channel_id=1, replica_groups=mesh['kv_0'=8,'kv_1'=8,'tp'=8] {'tp'}, dimensions={0} | all-to-all | bytes 32768 | tf_op jit(solution)/shard_map/all_to_all | solution.py:32
  127.6 0.3 all_to_all.30
  128.0 16.5 %all_to_all.41 = f32[64,1,705]{2,1,0:T(1,128)S(1)} all-to-all(f32[64,1,705]{2,1,0:T(1,128)S(1)} %all_to_all.30), channel_id=1, replica_groups=mesh['kv_0'=8,'kv_1'=8,'tp'=8] {'kv_0','kv_1'}, dimensions={0} | all-to-all | bytes 360960 | tf_op jit(solution)/shard_map/all_to_all | solution.py:21
  144.8 17.1 %all_to_all.42 = f32[64,1,705]{2,1,0:T(1,128)S(1)} all-to-all(f32[64,1,705]{2,1,0:T(1,128)S(1)} %broadcast_in_dim.31), channel_id=1, replica_groups=mesh['kv_0'=8,'kv_1'=8,'tp'=8] {'kv_0','kv_1'}, dimensions={0} | all-to-all | bytes 360960 | tf_op jit(solution)/shard_map/all_to_all | solution.py:32
  161.9 0.5 reduce.20
  162.3 0.2 reshape.1355
  162.7 0.2 convolution_convert_fusion
  163.1 9.8 %all_to_all.43 = bf16[8,2,512]{2,1,0:T(2,128)(2,1)S(1)} all-to-all(bf16[8,2,512]{2,1,0:T(2,128)(2,1)S(1)} %reshape.1515), channel_id=1, replica_groups=mesh['kv_0'=8,'kv_1'=8,'tp'=8] {'tp'}, dimensions={0} | all-to-all | bytes 32768 | tf_op jit(solution)/shard_map/all_to_all | solution.py:32
  173.0 0.6 fusion.51
  (113 shorter events, 6.9 us)
Async XLA Ops:
  0.0 54.8 %copy-start = (bf16[16,128,4,128]{3,2,1,0:T(4,128)(2,1)S(1)}, bf16[16,128,4,128]{3,2,1,0:T(4,128)(2,1)}, u32[]{:S(2)}) copy-start(bf16[16,128,4,128]{3,2,1,0:T(4,128)(2,1)} %param.21) | copy-start | bytes 6291460
  5.1 28.7 %all-to-all-start = ((f32[64,1,385]{2,1,0:T(1,128)}), f32[64,1,385]{2,1,0:T(1,128)S(1)}, u32[]{:S(2)}, u32[]{:S(2)}) async-start(f32[64,1,385]{2,1,0:T(1,128)} %all_to_all.26), calls=%async_computation | async-start | bytes 262144 | tf_op jit(solution)/shard_map/all_to_all | solution.py:21
  22.2 4.2 %copy-start.5 = (f32[4]{0:T(128)S(1)}, f32[4]{0:T(128)}, u32[]{:S(2)}) copy-start(f32[4]{0:T(128)} %param.23) | copy-start | bytes 52
  22.2 4.2 %copy-start.6 = (f32[128]{0:T(128)S(1)}, f32[128]{0:T(128)}, u32[]{:S(2)}) copy-start(f32[128]{0:T(128)} %param.24) | copy-start | bytes 1540
  22.2 17.2 %copy-start.7 = (s32[16]{0:T(128)S(1)}, s32[16]{0:T(128)}, u32[]{:S(2)}) copy-start(s32[16]{0:T(128)} %param.22) | copy-start | bytes 196
  34.6 16.4 %all-to-all-start.1 = ((f32[64,1,385]{2,1,0:T(1,128)}), f32[64,1,385]{2,1,0:T(1,128)S(1)}, u32[]{:S(2)}, u32[]{:S(2)}) async-start(f32[64,1,385]{2,1,0:T(1,128)} %broadcast_in_dim.27), calls=%async_computation.1 | async-start | bytes 262144 | tf_op jit(solution)/shard_map/all_to_all | solution.py:32
  75.1 27.2 %copy-start.9 = (bf16[512,64]{0,1:T(8,128)(2,1)S(1)}, bf16[512,64]{0,1:T(8,128)(2,1)}, u32[]{:S(2)}) copy-start(bf16[512,64]{0,1:T(8,128)(2,1)} %param.25) | copy-start | bytes 196612
  93.8 33.2 %copy-start.3 = (bf16[16,64]{1,0:T(8,128)(2,1)S(1)}, bf16[16,64]{1,0:T(8,128)(2,1)}, u32[]{:S(2)}) copy-start(bf16[16,64]{1,0:T(8,128)(2,1)} %param.15) | copy-start | bytes 6148
  93.8 33.3 %copy-start.1 = (bf16[64,1408]{1,0:T(8,128)(2,1)S(1)}, bf16[64,1408]{1,0:T(8,128)(2,1)}, u32[]{:S(2)}) copy-start(bf16[64,1408]{1,0:T(8,128)(2,1)} %param.27) | copy-start | bytes 540676
  93.8 33.3 %copy-start.4 = (f32[64]{0:T(128)S(1)}, f32[64]{0:T(128)}, u32[]{:S(2)}) copy-start(f32[64]{0:T(128)} %param.26) | copy-start | bytes 772
  94.7 32.6 %copy-start.2 = (bf16[64,1408]{1,0:T(8,128)(2,1)S(1)}, bf16[64,1408]{1,0:T(8,128)(2,1)}, u32[]{:S(2)}) copy-start(bf16[64,1408]{1,0:T(8,128)(2,1)} %param.28) | copy-start | bytes 540676
  127.3 35.4 %copy-start.8 = (bf16[1408,64]{0,1:T(8,128)(2,1)S(1)}, bf16[1408,64]{0,1:T(8,128)(2,1)}, u32[]{:S(2)}) copy-start(bf16[1408,64]{0,1:T(8,128)(2,1)} %param.29) | copy-start | bytes 540676
where the time goes:
time: 174 us
  blocking collectives  105 us (60%)
  starting transfers between devices  22 us (13%)
  waiting for transfers between devices  18.7 us (11%)
  local copies, waits for them, and re-layouts  14.9 us (9%)
  matrix products  6.57 us (4%)
  other arithmetic  5.63 us (3%)
    all_to_all x3, blocking collectives, from_everyone(): lax.all_to_all(jnp.broadcast_to(array[None], (devices, *array.shape)), ax...  51.2 us
    all_gather x2, blocking collectives, all_in_one(): both, at, found = (lax.all_gather(jnp.concatenate(lines), axis), 0, {})  37.4 us
    all_to_all x1, starting transfers between devices, summed_on_arrival(): lax.all_to_all(cut_along(array, dim, devices), axis, 0, 0, tiled=True)  17.1 us
    all_to_all x1, blocking collectives, summed_on_arrival(): lax.all_to_all(cut_along(array, dim, devices), axis, 0, 0, tiled=True)  16.5 us
    all_to_all x1, waiting for transfers between devices, from_everyone(): lax.all_to_all(jnp.broadcast_to(array[None], (devices, *array.shape)), ax...  11.5 us
    all_to_all x1, waiting for transfers between devices, summed_on_arrival(): lax.all_to_all(cut_along(array, dim, devices), axis, 0, 0, tiled=True)  7.25 us
    all_to_all x1, starting transfers between devices, from_everyone(): lax.all_to_all(jnp.broadcast_to(array[None], (devices, *array.shape)), ax...  4.89 us
    unnamed x28, local copies, waits for them, and re-layouts  4.64 us
  transfers between devices with their start and end apart: 2, of which 2 were waited for; matrix products, arithmetic and copies ran while one was open for 2% of the time, Pallas kernels for 0%

commit v1 on v0

v1 whole, which is shorter than its diff:
```python
import jax
import jax.numpy as jnp
from jax import lax
from jax.experimental import pallas as pl
from jax.experimental.pallas import tpu as pltpu
from jax.sharding import Mesh
from jax.sharding import PartitionSpec as P

KV = ("z", "y")
EPS = 1e-06
FLOOR_SCORE = -1e30
BF = jnp.bfloat16
F32 = jnp.float32
VMEM = pl.BlockSpec(memory_space=pltpu.VMEM)
SMEM = pl.BlockSpec(memory_space=pltpu.SMEM)
INTERPRET = False


def run(kernel, outs, args, scalars=0, scratch=()):
    single = not isinstance(outs, (list, tuple))
    return pl.pallas_call(
        kernel,
        out_shape=outs,
        in_specs=[SMEM] * scalars + [VMEM] * (len(args) - scalars),
        out_specs=VMEM if single else [VMEM] * len(outs),
        scratch_shapes=scratch,
        interpret=INTERPRET,
    )(*args)


def shape(*dims, kind=BF):
    return jax.ShapeDtypeStruct(dims, kind)


def exchange(array, axis):
    return lax.all_to_all(array, axis, 0, 0, tiled=True)


def dot(left, right):
    return jnp.dot(left, right, preferred_element_type=F32)


def dot_t(left, right):
    return lax.dot_general(left, right, (((1,), (1,)), ((), ())), preferred_element_type=F32)


def rounded(array):
    return array.astype(BF).astype(F32)


def summed(ref):
    total = ref[0].astype(F32)
    for i in range(1, ref.shape[0]):
        total = total + ref[i].astype(F32)
    return total


def iota(shape_, dim):
    return lax.broadcasted_iota(jnp.int32, shape_, dim)


def project(tokens, gain, w_query, w_key, w_value, out):
    x = tokens[...].astype(F32)
    scaled = (x * gain[...]).astype(BF)
    query = dot(scaled, w_query[...]).astype(BF)
    key = dot(scaled, w_key[...])
    value = dot(scaled, w_value[...])
    squares = jnp.broadcast_to(jnp.sum(x * x, axis=1, keepdims=True), (16, 128)).astype(BF)
    for y in range(8):
        rows = slice(8 * (y // 4), 8 * (y // 4) + 8)
        lanes = slice(128 * (y % 4), 128 * (y % 4) + 128)
        out[y, :, 0:512] = query
        out[y, :, 512:640] = jnp.concatenate([key[rows, lanes], value[rows, lanes]], axis=0).astype(BF)
        out[y, :, 640:768] = squares


def relay(got, out):
    total = summed(got).astype(BF)
    for i in range(8):
        out[i] = total


def attend(place, lengths, got, keys, values, out, rows_q, rows_k, rows_v, acc, stat):
    z, half, head = place[0], place[1] // 4, place[1] % 4
    start = (place[0] * 8 + place[1]) * 128
    total = summed(got)
    inverse = lax.rsqrt(total[:, 640:768] / 4096 + EPS)
    first = iota((16, 128), 1) < 64
    for h in range(4):
        query = rounded(inverse * total[:, 128 * h : 128 * h + 128])
        rows_q[pl.ds(2 * h, 16, stride=8), :] = jnp.where(first, query, 0.0)
        rows_q[pl.ds(2 * h + 1, 16, stride=8), :] = jnp.where(first, 0.0, query)
    inverse_half = jnp.where(half == 0, inverse[0:8], inverse[8:16])
    key_new = rounded(inverse_half * total[0:8, 512:640])
    value_new = rounded(inverse_half * total[8:16, 512:640])
    for part in range(2):
        for h in range(4):
            mine = jnp.logical_and(z == 0, jnp.logical_and(half == part, head == h))
            for m in range(2):
                at = pl.ds(64 * part + 2 * h + m, 8, stride=8)
                rows_k[at, :] = jnp.where(mine, key_new, 0.0)
                rows_v[at, :] = jnp.where(mine, value_new, 0.0)
    row = iota((8, 512), 0)
    column = iota((8, 512), 1)
    same_head = (column & 3) == (row >> 1)
    position = column >> 2
    owner_row = jnp.logical_and(z == 0, (iota((8, 1), 0) >> 1) == head)
    lane = iota((8, 128), 1)
    for b in range(16):
        at = slice(8 * b, 8 * b + 8)
        query = rows_q[at, :]
        scores = dot_t(query.astype(BF), keys[b]) * 0.125
        visible = jnp.logical_and(same_head, position < lengths[b] - start)
        scores = jnp.where(visible, scores, FLOOR_SCORE)
        owner = jnp.logical_and(owner_row, half == b // 8)
        own = jnp.sum(query * rows_k[at, :], axis=1, keepdims=True) * 0.125
        own = jnp.where(owner, own, FLOOR_SCORE)
        peak = jnp.maximum(jnp.max(scores, axis=1, keepdims=True), own)
        peak_hi = rounded(peak)
        peak_lo = rounded(peak - peak_hi)
        base = peak_hi + peak_lo
        weights = jnp.where(visible, jnp.exp(scores - base), 0.0)
        own_weight = jnp.where(owner, jnp.exp(own - base), 0.0)
        totals = jnp.sum(weights, axis=1, keepdims=True) + own_weight
        acc[at, :] = dot(weights.astype(BF), values[b]) + rounded(own_weight) * rows_v[at, :]
        totals_hi = rounded(totals)
        stat[at, :] = jnp.where(
            lane == 0,
            peak_hi,
            jnp.where(lane == 1, peak_lo, jnp.where(lane == 2, totals_hi, totals - totals_hi)),
        )
    body = acc[...].T.astype(BF)
    tail = stat[...].T[0:8].astype(BF)
    for i in range(8):
        out[i, 0:128, :] = body
        out[i, 128:136, :] = tail


def merged(got):
    tails = [got[i, 128:136, :].astype(F32) for i in range(8)]
    peaks = [t[0:1] + t[1:2] for t in tails]
    peak = peaks[0]
    for p in peaks[1:]:
        peak = jnp.maximum(peak, p)
    totals = jnp.zeros_like(peak)
    values = jnp.zeros((128, 128), F32)
    for i in range(8):
        scale = jnp.exp(peaks[i] - peak)
        totals = totals + scale * (tails[i][2:3] + tails[i][3:4])
        values = values + scale * got[i, 0:128, :].astype(F32)
    return peak, totals, values


def merge(got, out):
    peak, totals, values = merged(got)
    peak_hi, totals_hi = rounded(peak), rounded(totals)
    row = iota((8, 128), 0)
    tail = jnp.where(
        row == 0,
        peak_hi,
        jnp.where(row == 1, peak - peak_hi, jnp.where(row == 2, totals_hi, totals - totals_hi)),
    ).astype(BF)
    body = values.astype(BF)
    for i in range(8):
        out[i, 0:128, :] = body
        out[i, 128:136, :] = tail


def mix(weight, got, head_gain, w_out, out, rows):
    _, totals, values = merged(got)
    ratio = values / totals
    head = (iota((1, 128), 1) >> 1) & 3
    share = jnp.where(
        head == 0, weight[0], jnp.where(head == 1, weight[1], jnp.where(head == 2, weight[2], weight[3]))
    )
    mixture = ratio - share * pltpu.roll(ratio, 127, 1)
    scale = lax.rsqrt(jnp.mean(mixture * mixture, axis=0, keepdims=True) + EPS)
    rows[...] = (mixture * scale).T * head_gain[...]
    attended = jnp.concatenate(
        [rows[pl.ds(2 * h, 16, stride=8), :] for h in range(4)], axis=1
    ).astype(BF)
    term = dot_t(attended, w_out[...]).astype(BF)
    for i in range(8):
        out[i] = term


def widen(got, tokens, gain, w_gate, w_up, out, residual_out, rows):
    residual = (tokens[...].astype(F32) + summed(got)).astype(BF)
    residual_out[...] = residual
    x = residual.astype(F32)
    scaled = (x * gain[...]).astype(BF)
    gate = dot(scaled, w_gate[...])
    up = dot(scaled, w_up[...])
    squares = jnp.broadcast_to(jnp.sum(x * x, axis=1, keepdims=True), (16, 128))
    zeros = jnp.zeros((16, 128), F32)
    for tile in range(12):
        group, j = tile // 3, tile % 3
        lanes = slice(128 * tile, 128 * tile + 128)
        rows[pl.ds(8 * group + j, 16, stride=32), :] = gate[:, lanes] if tile < 11 else zeros
        rows[pl.ds(8 * group + 3 + j, 16, stride=32), :] = up[:, lanes] if tile < 11 else zeros
    for group in range(4):
        rows[pl.ds(8 * group + 6, 16, stride=32), :] = squares
        rows[pl.ds(8 * group + 7, 16, stride=32), :] = squares
    out[...] = rows[...].astype(BF)


def activate(got, out):
    total = summed(got)
    inverse = lax.rsqrt(total[6:7] / 4096 + EPS)
    gate = inverse * total[0:3]
    up = inverse * total[3:6]
    hidden = gate / (1.0 + jnp.exp(-gate)) * up
    hidden = jnp.concatenate([hidden, jnp.zeros((5, 128), F32)], axis=0).astype(BF)
    for i in range(64):
        out[i] = hidden


def narrow(got, w_down, out, rows):
    rows[...] = got[...].astype(F32)
    hidden = jnp.concatenate(
        [rows[pl.ds(8 * (t // 3) + t % 3, 16, stride=32), :] for t in range(11)], axis=1
    ).astype(BF)
    term = dot_t(hidden, w_down[...]).astype(BF)
    for i in range(8):
        out[i] = term


def local(
    tokens,
    attn_gain,
    w_query,
    w_key,
    w_value,
    key_cache,
    value_cache,
    lengths,
    mix_weight,
    head_gain,
    w_out,
    mixer_gain,
    w_gate,
    w_up,
    w_down,
):
    place = jnp.stack([lax.axis_index("z"), lax.axis_index("y")]).astype(jnp.int32)
    tile = pltpu.VMEM((128, 128), F32)
    wide = pltpu.VMEM((512, 128), F32)
    sent = run(project, shape(8, 16, 768), (tokens, attn_gain[None], w_query, w_key, w_value))
    sent = run(relay, shape(8, 16, 768), (exchange(sent, "y"),))
    sent = run(
        attend,
        shape(8, 136, 128),
        (
            place,
            lengths,
            exchange(sent, "z"),
            key_cache.reshape(16, 512, 128),
            value_cache.reshape(16, 512, 128),
        ),
        scalars=2,
        scratch=[tile] * 5,
    )
    sent = run(merge, shape(8, 136, 128), (exchange(sent, "y"),))
    sent = run(
        mix,
        shape(8, 16, 64),
        (mix_weight, exchange(sent, "z"), head_gain[None], w_out.T),
        scalars=1,
        scratch=[tile],
    )
    sent, residual = run(
        widen,
        (shape(512, 128), shape(16, 64)),
        (exchange(sent, "tp"), tokens, mixer_gain[None], w_gate, w_up),
        scratch=[wide],
    )
    sent = run(activate, shape(64, 8, 128), (exchange(sent.reshape(64, 8, 128), KV),))
    sent = run(
        narrow, shape(8, 16, 64), (exchange(sent, KV).reshape(512, 128), w_down.T), scratch=[wide]
    )
    terms = exchange(sent, "tp")
    return (residual.astype(F32) + jnp.sum(terms.astype(F32), axis=0)).astype(BF)


def solution(mesh):
    finer = Mesh(mesh.devices.reshape(8, 8, mesh.shape["tp"]), ("z", "y", "tp"))
    return jax.shard_map(
        local,
        mesh=finer,
        in_specs=(
            P(None, KV),
            P(KV),
            P(KV, "tp"),
            P(KV, "tp"),
            P(KV, "tp"),
            P(None, KV, "tp", None),
            P(None, KV, "tp", None),
            P(),
            P("tp"),
            P(),
            P("tp", KV),
            P(KV),
            P(KV, "tp"),
            P(KV, "tp"),
            P("tp", KV),
        ),
        out_specs=P(None, KV),
        check_vma=False,
    )
```

time: 174 us -> 146 us (0.84)
  Pallas kernels: 0 us -> 19.6 us
  local copies, waits for them, and re-layouts: 14.9 us -> 3.18 us
  starting transfers between devices: 22 us -> 10.3 us
  waiting for transfers between devices: 18.7 us -> 8.11 us
  matrix products: 6.57 us -> 0 us
  other arithmetic: 5.63 us -> 1.92 us
  blocking collectives: 105 us -> 102 us
    all_gather x2 -> x0, blocking collectives: 37.4 us -> none  [all_in_one(): both, at, found = (lax.all_gather(jnp.concatenate(lines), axis), 0, {})]
    all_to_all x4 -> x7, blocking collectives: 67.7 us -> 102 us  [exchange(): return lax.all_to_all(array, axis, 0, 0, tiled=True)]
    pallas_call x0 -> x8, Pallas kernels: none -> 19.6 us  [run(): pl.pallas_call(kernel, out_shape=outs, in_specs=[SMEM] * scalars + [VMEM]...]
    all_to_all x2 -> x1, starting transfers between devices: 22 us -> 10.3 us  [exchange(): return lax.all_to_all(array, axis, 0, 0, tiled=True)]
    all_to_all x2 -> x1, waiting for transfers between devices: 18.7 us -> 8.11 us  [exchange(): return lax.all_to_all(array, axis, 0, 0, tiled=True)]
    dot_general x9 -> x0, matrix products: 6.57 us -> none  [the longest x1 2.24 us: local(): jnp.einsum('bhmd,bphmd->bhmp', queries, cached_keys, preferred_element_ty...]
    convert_element_type x35 -> x0, local copies, waits for them, and re-layouts: 4.72 us -> none  [the longest x32 4.31 us: joined_all(): part[k].astype(own.dtype)]
    reduce_sum x9 -> x1, other arithmetic: 2.09 us -> 0.01 us  [local(): jnp.sum(terms.astype(F32), axis=0)]
  transfers between devices with their start and end apart: 2 -> 1, of which waited for: 2 -> 1; matrix products, arithmetic and copies ran while one was open for 2% -> 0% of each run, Pallas kernels for 0% -> 0%
where the time goes in v1:
time: 146 us; the launch traced here: 145 us
  blocking collectives  102 us (70%)
  Pallas kernels  19.6 us (13%)
  starting transfers between devices  10.3 us (7%)
  waiting for transfers between devices  8.11 us (6%)
  local copies, waits for them, and re-layouts  3.18 us (2%)
  other arithmetic  1.92 us (1%)
    all_to_all x7, blocking collectives, exchange(): return lax.all_to_all(array, axis, 0, 0, tiled=True)  102 us
    pallas_call x8, Pallas kernels, run(): pl.pallas_call(kernel, out_shape=outs, in_specs=[SMEM] * scalars + [VMEM]...  19.6 us
    all_to_all x1, starting transfers between devices, exchange(): return lax.all_to_all(array, axis, 0, 0, tiled=True)  10.3 us
    all_to_all x1, waiting for transfers between devices, exchange(): return lax.all_to_all(array, axis, 0, 0, tiled=True)  8.11 us
    unnamed x6, local copies, waits for them, and re-layouts  3.18 us
  transfers between devices with their start and end apart: 1, of which 1 were waited for; matrix products, arithmetic and copies ran while one was open for 0% of the time, Pallas kernels for 0%

profile of v1, /device:TPU:1, one launch (start us, length us, event | category | flops | bytes accessed | tf_op | source)
XLA Modules:
  0.0 145.4 jit_solution(442535566627338127)
XLA Ops:
  0.0 1.7 %shard_map.145 = bf16[8,16,768]{2,1,0:T(8,128)(2,1)} custom-call(bf16[16,64]{1,0:T(8,128)(2,1)} %tokens.3, f32[1,64]{1,0:T(1,128)} %bitcast.17, bf16[64,512]{1,0:T(8,128)(2,1)} %w_query.1, bf16[64,512]{1,0:T(8,128)(2,1)} %w_key.1, bf16[64,512]{1,0:T(8,128)(2,1)} %w_value.1), custom_call_target="tpu_custom_call" | custom-call | tf_op jit(solution)/shard_map/pallas_call | solution.py:21
  1.7 16.5 %all_to_all.40.got = bf16[8,16,768]{2,1,0:T(8,128)(2,1)} all-to-all(bf16[8,16,768]{2,1,0:T(8,128)(2,1)} %shard_map.145), channel_id=1, replica_groups=mesh['z'=8,'y'=8,'tp'=8] {'y'}, dimensions={0} | all-to-all | bytes 393216 | tf_op jit(solution)/shard_map/all_to_all | solution.py:36
  18.2 1.6 %shard_map.146 = bf16[8,16,768]{2,1,0:T(8,128)(2,1)} custom-call(bf16[8,16,768]{2,1,0:T(8,128)(2,1)} %all_to_all.40.got), custom_call_target="tpu_custom_call" | custom-call | tf_op jit(solution)/shard_map/pallas_call | solution.py:21
  19.8 10.3 %all-to-all-start.1 = ((bf16[8,16,768]{2,1,0:T(8,128)(2,1)}), bf16[8,16,768]{2,1,0:T(8,128)(2,1)S(1)}, u32[]{:S(2)}, u32[]{:S(2)}) async-start(bf16[8,16,768]{2,1,0:T(8,128)(2,1)} %shard_map.146), calls=%async_computation.1 | async-start | bytes 393216 | tf_op jit(solution)/shard_map/all_to_all | solution.py:36
  30.1 0.6 pad_add_fusion.place
  30.8 8.1 %all-to-all-done.1.got = bf16[8,16,768]{2,1,0:T(8,128)(2,1)S(1)} async-done(((bf16[8,16,768]{2,1,0:T(8,128)(2,1)}), bf16[8,16,768]{2,1,0:T(8,128)(2,1)S(1)}, u32[]{:S(2)}, u32[]{:S(2)}) %all-to-all-start.1) | async-done | bytes 196640 | tf_op jit(solution)/shard_map/all_to_all | solution.py:36
  38.9 0.0 copy-start
  38.9 0.7 copy-done
  39.6 7.1 %shard_map.147 = bf16[8,136,128]{2,1,0:T(8,128)(2,1)} custom-call(s32[2]{0:T(128)} %pad_add_fusion.place, s32[16]{0:T(128)} %lengths.1, bf16[8,16,768]{2,1,0:T(8,128)(2,1)} %copy-done, bf16[16,512,128]{2,1,0:T(8,128)(2,1)} %bitcast.11, bf16[16,512,128]{2,1,0:T(8,128)(2,1)} %bitcast.12), custom_call_target="tpu_custom_call" | custom-call | tf_op jit(solution)/shard_map/pallas_call | solution.py:21
  46.7 13.6 %all_to_all.41.got = bf16[8,136,128]{2,1,0:T(8,128)(2,1)} all-to-all(bf16[8,136,128]{2,1,0:T(8,128)(2,1)} %shard_map.147), channel_id=1, replica_groups=mesh['z'=8,'y'=8,'tp'=8] {'y'}, dimensions={0} | all-to-all | bytes 557056 | tf_op jit(solution)/shard_map/all_to_all | solution.py:36
  60.2 1.7 %shard_map.148 = bf16[8,136,128]{2,1,0:T(8,128)(2,1)} custom-call(bf16[8,136,128]{2,1,0:T(8,128)(2,1)} %all_to_all.41.got), custom_call_target="tpu_custom_call" | custom-call | tf_op jit(solution)/shard_map/pallas_call | solution.py:21
  62.0 13.6 %all_to_all.42.got = bf16[8,136,128]{2,1,0:T(8,128)(2,1)} all-to-all(bf16[8,136,128]{2,1,0:T(8,128)(2,1)} %shard_map.148), channel_id=1, replica_groups=mesh['z'=8,'y'=8,'tp'=8] {'z'}, dimensions={0} | all-to-all | bytes 557056 | tf_op jit(solution)/shard_map/all_to_all | solution.py:36
  75.5 2.0 %shard_map.149 = bf16[8,16,64]{2,1,0:T(8,128)(2,1)} custom-call(f32[4]{0:T(128)} %weight.1, bf16[8,136,128]{2,1,0:T(8,128)(2,1)} %all_to_all.42.got, f32[1,128]{1,0:T(1,128)} %bitcast.18, bf16[64,512]{1,0:T(8,128)(2,1)} %bitcast.16), custom_call_target="tpu_custom_call" | custom-call | tf_op jit(solution)/shard_map/pallas_call | solution.py:21
  77.5 0.8 reshape.16
  78.3 14.8 %all_to_all.43 = bf16[8,2,512]{2,1,0:T(2,128)(2,1)S(1)} all-to-all(bf16[8,2,512]{2,1,0:T(2,128)(2,1)S(1)} %reshape.16), channel_id=1, replica_groups=mesh['z'=8,'y'=8,'tp'=8] {'tp'}, dimensions={0} | all-to-all | bytes 32768 | tf_op jit(solution)/shard_map/all_to_all | solution.py:36
  93.1 0.7 reshape.17.got
  93.8 2.0 %shard_map.150 = (bf16[512,128]{1,0:T(8,128)(2,1)}, bf16[16,64]{1,0:T(8,128)(2,1)}) custom-call(bf16[8,16,64]{2,1,0:T(8,128)(2,1)} %reshape.17.got, bf16[16,64]{1,0:T(8,128)(2,1)} %tokens.3, f32[1,64]{1,0:T(1,128)} %bitcast.19, bf16[64,1408]{1,0:T(8,128)(2,1)} %w_gate.1, bf16[64,1408]{1,0:T(8,128)(2,1)} %w_up.1), custom_call_target="tpu_custom_call" | custom-call | tf_op jit(solution)/shard_map/pallas_call | solution.py:21
  95.8 16.9 %all_to_all.44.got = bf16[64,8,128]{2,1,0:T(8,128)(2,1)} all-to-all(bf16[64,8,128]{2,1,0:T(8,128)(2,1)} %bitcast.15), channel_id=1, replica_groups=mesh['z'=8,'y'=8,'tp'=8] {'z','y'}, dimensions={0} | all-to-all | bytes 262144 | tf_op jit(solution)/shard_map/all_to_all | solution.py:36
  112.7 1.6 %shard_map.151 = bf16[64,8,128]{2,1,0:T(8,128)(2,1)} custom-call(bf16[64,8,128]{2,1,0:T(8,128)(2,1)} %all_to_all.44.got), custom_call_target="tpu_custom_call" | custom-call | tf_op jit(solution)/shard_map/pallas_call | solution.py:21
  114.3 16.9 %all_to_all.45 = bf16[64,8,128]{2,1,0:T(8,128)(2,1)} all-to-all(bf16[64,8,128]{2,1,0:T(8,128)(2,1)} %shard_map.151), channel_id=1, replica_groups=mesh['z'=8,'y'=8,'tp'=8] {'z','y'}, dimensions={0} | all-to-all | bytes 262144 | tf_op jit(solution)/shard_map/all_to_all | solution.py:36
  131.2 1.8 %shard_map.152 = bf16[8,16,64]{2,1,0:T(8,128)(2,1)} custom-call(bf16[512,128]{1,0:T(8,128)(2,1)} %bitcast.13, bf16[64,1408]{1,0:T(8,128)(2,1)} %bitcast.14), custom_call_target="tpu_custom_call" | custom-call | tf_op jit(solution)/shard_map/pallas_call | solution.py:21
  132.9 0.8 reshape.18
  133.8 10.2 %all_to_all.46 = bf16[8,2,512]{2,1,0:T(2,128)(2,1)S(1)} all-to-all(bf16[8,2,512]{2,1,0:T(2,128)(2,1)S(1)} %reshape.18), channel_id=1, replica_groups=mesh['z'=8,'y'=8,'tp'=8] {'tp'}, dimensions={0} | all-to-all | bytes 32768 | tf_op jit(solution)/shard_map/all_to_all | solution.py:36
  144.0 0.1 reshape.19
  144.1 1.3 add_convert_fusion
  (1 shorter events, 0.0 us)
Async XLA Ops:
  19.8 19.0 %all-to-all-start.1 = ((bf16[8,16,768]{2,1,0:T(8,128)(2,1)}), bf16[8,16,768]{2,1,0:T(8,128)(2,1)S(1)}, u32[]{:S(2)}, u32[]{:S(2)}) async-start(bf16[8,16,768]{2,1,0:T(8,128)(2,1)} %shard_map.146), calls=%async_computation.1 | async-start | bytes 393216 | tf_op jit(solution)/shard_map/all_to_all | solution.py:36
  38.9 0.7 copy-start

commit v2 on v1

v2 whole, which is shorter than its diff:
```python
import jax
import jax.numpy as jnp
from jax import lax
from jax.experimental import pallas as pl
from jax.experimental.pallas import tpu as pltpu
from jax.sharding import Mesh
from jax.sharding import PartitionSpec as P

KV = ("z", "y")
EPS = 1e-06
FLOOR_SCORE = -1e30
BF = jnp.bfloat16
F32 = jnp.float32
VMEM = pl.BlockSpec(memory_space=pltpu.VMEM)
HBM = pl.BlockSpec(memory_space=pltpu.HBM)
INTERPRET = False


def run(kernel, outs, args, specs=None, scratch=(), grant=4):
    single = not isinstance(outs, (list, tuple))
    specs = specs or [VMEM] * len(args)
    if not INTERPRET:
        args = [
            pltpu.with_memory_space_constraint(a, s.memory_space) for a, s in zip(args, specs)
        ]
    return pl.pallas_call(
        kernel,
        out_shape=outs,
        in_specs=specs,
        out_specs=VMEM if single else [VMEM] * len(outs),
        scratch_shapes=scratch,
        compiler_params=pltpu.CompilerParams(vmem_limit_bytes=grant << 20),
        interpret=INTERPRET,
    )(*args)


def shape(*dims, kind=BF):
    return jax.ShapeDtypeStruct(dims, kind) if INTERPRET else pltpu.VMEM(dims, kind)


def exchange(array, axis):
    return lax.all_to_all(array, axis, 0, 0, tiled=True)


def dot(left, right):
    return jnp.dot(left, right, preferred_element_type=F32)


def dot_t(left, right):
    return lax.dot_general(left, right, (((1,), (1,)), ((), ())), preferred_element_type=F32)


def rounded(array):
    return array.astype(BF).astype(F32)


def summed(ref):
    total = ref[0].astype(F32)
    for i in range(1, ref.shape[0]):
        total = total + ref[i].astype(F32)
    return total


def folded(term):
    return jnp.concatenate([term[0:8], term[8:16]], axis=1).astype(BF)


def unfolded(term):
    return jnp.concatenate([term[:, 0:64], term[:, 64:128]], axis=0)


def iota(shape_, dim):
    return lax.broadcasted_iota(jnp.int32, shape_, dim)


def project(
    tokens, gain, w_query, w_key, w_value, lengths, weight, keys, values,
    out, keys_out, values_out, limit, owner, share,
    tokens_in, gain_in, query_in, key_in, value_in, lengths_in, weight_in, sems,
):
    pairs = (
        (tokens, tokens_in),
        (gain, gain_in),
        (w_query, query_in),
        (w_key, key_in),
        (w_value, value_in),
        (lengths, lengths_in),
        (weight, weight_in),
        (keys, keys_out),
        (values, values_out),
    )
    copies = [pltpu.make_async_copy(a, b, sems.at[i]) for i, (a, b) in enumerate(pairs)]
    for copy in copies:
        copy.start()
    for copy in copies[:5]:
        copy.wait()
    x = tokens_in[...].astype(F32)
    scaled = (x * gain_in[...]).astype(BF)
    query = dot(scaled, query_in[...]).astype(BF)
    key = dot(scaled, key_in[...])
    value = dot(scaled, value_in[...])
    squares = jnp.broadcast_to(jnp.sum(x * x, axis=1, keepdims=True), (16, 128)).astype(BF)
    for y in range(8):
        rows = slice(8 * (y // 4), 8 * (y // 4) + 8)
        lanes = slice(128 * (y % 4), 128 * (y % 4) + 128)
        out[y, :, 0:512] = query
        out[y, :, 512:640] = jnp.concatenate([key[rows, lanes], value[rows, lanes]], axis=0).astype(BF)
        out[y, :, 640:768] = squares
    for copy in copies[5:7]:
        copy.wait()
    z, y = lax.axis_index("z"), lax.axis_index("y")
    half, head = y // 4, y % 4
    start = (z * 8 + y) * 128
    row_head = iota((8, 128), 0) >> 1
    same_head = (iota((8, 128), 1) & 3) == row_head
    for b in range(16):
        at = slice(8 * b, 8 * b + 8)
        limit[at, :] = jnp.where(same_head, lengths_in[b] - start, 0)
        mine = jnp.logical_and(z == 0, half == b // 8)
        owner[at, :] = jnp.where(jnp.logical_and(mine, row_head == head), 1, 0)
    lane_head = (iota((8, 128), 1) >> 1) & 3
    low = jnp.where(lane_head == 0, weight_in[0], weight_in[1])
    high = jnp.where(lane_head == 2, weight_in[2], weight_in[3])
    share[...] = jnp.where(lane_head < 2, low, high)
    for copy in copies[7:]:
        copy.wait()


def relay(got, out):
    total = summed(got).astype(BF)
    for i in range(8):
        out[i] = total


def attend(got, keys, values, limit, owner, out, rows_q, rows_k, rows_v, scores, acc):
    total = summed(got)
    inverse = lax.rsqrt(total[:, 640:768] / 4096 + EPS)
    first = iota((16, 128), 1) < 64
    for h in range(4):
        query = rounded(inverse * total[:, 128 * h : 128 * h + 128])
        rows_q[pl.ds(2 * h, 16, stride=8), :] = jnp.where(first, query, 0.0)
        rows_q[pl.ds(2 * h + 1, 16, stride=8), :] = jnp.where(first, 0.0, query)
    for b in range(16):
        at = slice(8 * b, 8 * b + 8)
        scores[at, :] = dot_t(rows_q[at, :].astype(BF), keys[b])
    for part in range(2):
        scale = inverse[8 * part : 8 * part + 8]
        key_new = rounded(scale * total[0:8, 512:640])
        value_new = rounded(scale * total[8:16, 512:640])
        for i in range(8):
            at = pl.ds(64 * part + i, 8, stride=8)
            rows_k[at, :] = key_new
            rows_v[at, :] = value_new
    owned = owner[...] > 0
    own = jnp.sum(rows_q[...] * rows_k[...], axis=1, keepdims=True) * 0.125
    own = jnp.where(owned, own, FLOOR_SCORE)
    lane = iota((128, 128), 1)
    tiles, seen = [], []
    peak = own
    for t in range(4):
        visible = (lane + 128 * t) >> 2 < limit[...]
        tile = jnp.where(visible, scores[:, 128 * t : 128 * t + 128] * 0.125, FLOOR_SCORE)
        tiles.append(tile)
        seen.append(visible)
        peak = jnp.maximum(peak, tile)
    peak = jnp.max(peak, axis=1, keepdims=True)
    peak_hi = rounded(peak)
    peak_lo = rounded(peak - peak_hi)
    base = peak_hi + peak_lo
    weights = [jnp.where(v, jnp.exp(t - base), 0.0) for t, v in zip(tiles, seen)]
    own_weight = jnp.where(owned, jnp.exp(own - base), 0.0)
    totals = jnp.sum(weights[0] + weights[1] + weights[2] + weights[3], axis=1, keepdims=True)
    totals = totals + own_weight
    weights = jnp.concatenate(weights, axis=1).astype(BF)
    for b in range(16):
        at = slice(8 * b, 8 * b + 8)
        acc[at, :] = dot(weights[at, :], values[b])
    body = (acc[...] + rounded(own_weight) * rows_v[...]).T.astype(BF)
    totals_hi = rounded(totals)
    stat = jnp.where(
        lane == 0,
        peak_hi,
        jnp.where(lane == 1, peak_lo, jnp.where(lane == 2, totals_hi, totals - totals_hi)),
    )
    tail = stat.T[0:8].astype(BF)
    for i in range(8):
        out[i, 0:128, :] = body
        out[i, 128:136, :] = tail


def merged(got):
    tails = [got[i, 128:136, :].astype(F32) for i in range(8)]
    peaks = [t[0:1] + t[1:2] for t in tails]
    peak = peaks[0]
    for p in peaks[1:]:
        peak = jnp.maximum(peak, p)
    totals = jnp.zeros_like(peak)
    values = jnp.zeros((128, 128), F32)
    for i in range(8):
        scale = jnp.exp(peaks[i] - peak)
        totals = totals + scale * (tails[i][2:3] + tails[i][3:4])
        values = values + scale * got[i, 0:128, :].astype(F32)
    return peak, totals, values


def merge(got, out):
    peak, totals, values = merged(got)
    peak_hi, totals_hi = rounded(peak), rounded(totals)
    row = iota((8, 128), 0)
    tail = jnp.where(
        row == 0,
        peak_hi,
        jnp.where(row == 1, peak - peak_hi, jnp.where(row == 2, totals_hi, totals - totals_hi)),
    ).astype(BF)
    body = values.astype(BF)
    for i in range(8):
        out[i, 0:128, :] = body
        out[i, 128:136, :] = tail


def mix(got, share, head_gain, w_out, out, rows):
    _, totals, values = merged(got)
    ratio = values / totals
    mixture = ratio - share[0:1] * pltpu.roll(ratio, 127, 1)
    scale = lax.rsqrt(jnp.mean(mixture * mixture, axis=0, keepdims=True) + EPS)
    rows[...] = (mixture * scale).T * head_gain[...]
    attended = jnp.concatenate(
        [rows[pl.ds(2 * h, 16, stride=8), :] for h in range(4)], axis=1
    ).astype(BF)
    term = folded(dot_t(attended, w_out[...]))
    for i in range(8):
        out[i] = term


def widen(got, tokens, gain, w_gate, w_up, out, residual_out, rows):
    residual = (tokens[...].astype(F32) + unfolded(summed(got))).astype(BF)
    residual_out[...] = residual
    x = residual.astype(F32)
    scaled = (x * gain[...]).astype(BF)
    gate = dot(scaled, w_gate[...])
    up = dot(scaled, w_up[...])
    squares = jnp.broadcast_to(jnp.sum(x * x, axis=1, keepdims=True), (16, 128))
    zeros = jnp.zeros((16, 128), F32)
    for tile in range(12):
        group, j = tile // 3, tile % 3
        lanes = slice(128 * tile, 128 * tile + 128)
        rows[pl.ds(8 * group + j, 16, stride=32), :] = gate[:, lanes] if tile < 11 else zeros
        rows[pl.ds(8 * group + 3 + j, 16, stride=32), :] = up[:, lanes] if tile < 11 else zeros
    for group in range(4):
        rows[pl.ds(8 * group + 6, 16, stride=32), :] = squares
        rows[pl.ds(8 * group + 7, 16, stride=32), :] = squares
    out[...] = rows[...].astype(BF)


def activate(got, out):
    total = summed(got)
    inverse = lax.rsqrt(total[6:7] / 4096 + EPS)
    gate = inverse * total[0:3]
    up = inverse * total[3:6]
    hidden = gate / (1.0 + jnp.exp(-gate)) * up
    hidden = jnp.concatenate([hidden, jnp.zeros((5, 128), F32)], axis=0).astype(BF)
    for i in range(64):
        out[i] = hidden


def narrow(got, w_down, out, rows):
    rows[...] = got[...].astype(F32)
    hidden = jnp.concatenate(
        [rows[pl.ds(8 * (t // 3) + t % 3, 16, stride=32), :] for t in range(11)], axis=1
    ).astype(BF)
    term = folded(dot_t(hidden, w_down[...]))
    for i in range(8):
        out[i] = term


def finish(got, residual, out):
    out[...] = (residual[...].astype(F32) + unfolded(summed(got))).astype(BF)


def local(
    tokens,
    attn_gain,
    w_query,
    w_key,
    w_value,
    key_cache,
    value_cache,
    lengths,
    mix_weight,
    head_gain,
    w_out,
    mixer_gain,
    w_gate,
    w_up,
    w_down,
):
    tile = pltpu.VMEM((128, 128), F32)
    wide = pltpu.VMEM((512, 128), F32)
    sent, keys, values, limit, owner, share = run(
        project,
        (
            shape(8, 16, 768),
            shape(16, 512, 128),
            shape(16, 512, 128),
            shape(128, 128, kind=jnp.int32),
            shape(128, 128, kind=jnp.int32),
            shape(8, 128, kind=F32),
        ),
        (
            tokens,
            attn_gain[None],
            w_query,
            w_key,
            w_value,
            lengths,
            mix_weight,
            key_cache.reshape(16, 512, 128),
            value_cache.reshape(16, 512, 128),
        ),
        specs=[HBM] * 9,
        scratch=[
            pltpu.VMEM((16, 64), BF),
            pltpu.VMEM((1, 64), F32),
            pltpu.VMEM((64, 512), BF),
            pltpu.VMEM((64, 512), BF),
            pltpu.VMEM((64, 512), BF),
            pltpu.SMEM((16,), jnp.int32),
            pltpu.SMEM((4,), F32),
            pltpu.SemaphoreType.DMA((9,)),
        ],
    )
    sent = run(relay, shape(8, 16, 768), (exchange(sent, "y"),))
    sent = run(
        attend,
        shape(8, 136, 128),
        (exchange(sent, "z"), keys, values, limit, owner),
        scratch=[tile, tile, tile, pltpu.VMEM((128, 512), F32), tile],
    )
    sent = run(merge, shape(8, 136, 128), (exchange(sent, "y"),))
    sent = run(
        mix,
        shape(8, 8, 128),
        (exchange(sent, "z"), share, head_gain[None], w_out.T),
        scratch=[tile],
    )
    sent, residual = run(
        widen,
        (shape(512, 128), shape(16, 64)),
        (exchange(sent, "tp"), tokens, mixer_gain[None], w_gate, w_up),
        scratch=[wide],
    )
    sent = run(activate, shape(64, 8, 128), (exchange(sent.reshape(64, 8, 128), KV),))
    sent = run(
        narrow, shape(8, 8, 128), (exchange(sent, KV).reshape(512, 128), w_down.T), scratch=[wide]
    )
    return run(finish, jax.ShapeDtypeStruct((16, 64), BF), (exchange(sent, "tp"), residual))


def solution(mesh):
    finer = Mesh(mesh.devices.reshape(8, 8, mesh.shape["tp"]), ("z", "y", "tp"))
    return jax.shard_map(
        local,
        mesh=finer,
        in_specs=(
            P(None, KV),
            P(KV),
            P(KV, "tp"),
            P(KV, "tp"),
            P(KV, "tp"),
            P(None, KV, "tp", None),
            P(None, KV, "tp", None),
            P(),
            P("tp"),
            P(),
            P("tp", KV),
            P(KV),
            P(KV, "tp"),
            P(KV, "tp"),
            P("tp", KV),
        ),
        out_specs=P(None, KV),
        check_vma=False,
    )
```

time: 146 us -> 121 us (0.83)
  Pallas kernels: 19.6 us -> 5.42 us
  blocking collectives: 102 us -> 115 us
  starting transfers between devices: 10.3 us -> 0 us
  waiting for transfers between devices: 8.11 us -> 0 us
  local copies, waits for them, and re-layouts: 3.18 us -> 0.03 us
  other arithmetic: 1.92 us -> 0 us
    pallas_call x8 -> x9, Pallas kernels: 19.6 us -> 5.42 us  [run(): pl.pallas_call(kernel, out_shape=outs, in_specs=specs, out_specs=VMEM if...]
    all_to_all x7 -> x8, blocking collectives: 102 us -> 115 us  [exchange(): return lax.all_to_all(array, axis, 0, 0, tiled=True)]
    all_to_all x1 -> x0, starting transfers between devices: 10.3 us -> none  [exchange(): return lax.all_to_all(array, axis, 0, 0, tiled=True)]
    all_to_all x1 -> x0, waiting for transfers between devices: 8.11 us -> none  [exchange(): return lax.all_to_all(array, axis, 0, 0, tiled=True)]
    unnamed x6 -> x14, local copies, waits for them, and re-layouts: 3.18 us -> 0.03 us
  transfers between devices with their start and end apart: 1 -> 0, of which waited for: 1 -> 0; matrix products, arithmetic and copies ran while one was open for 0% -> 0% of each run, Pallas kernels for 0% -> 0%
where the time goes in v2:
time: 121 us; the launch traced here: 120 us
  blocking collectives  115 us (95%)
  Pallas kernels  5.42 us (4%)
    all_to_all x8, blocking collectives, exchange(): return lax.all_to_all(array, axis, 0, 0, tiled=True)  115 us
    pallas_call x9, Pallas kernels, run(): pl.pallas_call(kernel, out_shape=outs, in_specs=specs, out_specs=VMEM if...  5.42 us

profile of v2, /device:TPU:1, one launch (start us, length us, event | category | flops | bytes accessed | tf_op | source)
XLA Modules:
  0.0 120.2 jit_solution(14807429197839179325)
XLA Ops:
  0.0 2.4 %shard_map.145 = (bf16[8,16,768]{2,1,0:T(8,128)(2,1)S(1)}, bf16[16,512,128]{2,1,0:T(8,128)(2,1)S(1)}, bf16[16,512,128]{2,1,0:T(8,128)(2,1)S(1)}, s32[128,128]{1,...) custom-call(bf16[16,64]{1,0:T(8,128)(2,1)} %tokens.3, f32[1,64]{1,0:T(1,128)} %bitcast.17, ...), custom_call_target="tpu_custom_call" | custom-call | tf_op jit(solution)/shard_map/pallas_call | solution.py:26
  2.5 16.2 %all_to_all.40.got = bf16[8,16,768]{2,1,0:T(8,128)(2,1)S(1)} all-to-all(bf16[8,16,768]{2,1,0:T(8,128)(2,1)S(1)} %get-tuple-element.13), channel_id=1, replica_groups=mesh['z'=8,'y'=8,'tp'=8] {'y'}, dimensions={0} | all-to-all | bytes 393216 | tf_op jit(solution)/shard_map/all_to_all | solution.py:42
  18.7 18.8 %all_to_all.41.got = bf16[8,16,768]{2,1,0:T(8,128)(2,1)S(1)} all-to-all(bf16[8,16,768]{2,1,0:T(8,128)(2,1)S(1)} %shard_map.146), channel_id=1, replica_groups=mesh['z'=8,'y'=8,'tp'=8] {'z'}, dimensions={0} | all-to-all | bytes 393216 | tf_op jit(solution)/shard_map/all_to_all | solution.py:42
  37.5 0.0 copy-start.3
  37.5 0.0 copy-start.5
  37.5 0.0 copy-start.4
  37.5 0.0 copy-start.6
  37.5 1.0 shard_map.147
  38.5 0.0 copy-start
  38.6 0.0 copy-start.1
  38.6 0.0 copy-start.2
  38.6 12.1 %all_to_all.42.got = bf16[8,136,128]{2,1,0:T(8,128)(2,1)S(1)} all-to-all(bf16[8,136,128]{2,1,0:T(8,128)(2,1)S(1)} %shard_map.147), channel_id=1, replica_groups=mesh['z'=8,'y'=8,'tp'=8] {'y'}, dimensions={0} | all-to-all | bytes 557056 | tf_op jit(solution)/shard_map/all_to_all | solution.py:42
  50.7 0.1 shard_map.148
  50.8 11.9 %all_to_all.43.got = bf16[8,136,128]{2,1,0:T(8,128)(2,1)S(1)} all-to-all(bf16[8,136,128]{2,1,0:T(8,128)(2,1)S(1)} %shard_map.148), channel_id=1, replica_groups=mesh['z'=8,'y'=8,'tp'=8] {'z'}, dimensions={0} | all-to-all | bytes 557056 | tf_op jit(solution)/shard_map/all_to_all | solution.py:42
  62.8 0.0 copy-done.3
  62.8 0.0 copy-done.5
  62.8 0.5 shard_map.149
  63.2 14.7 %all_to_all.44.got = bf16[8,8,128]{2,1,0:T(8,128)(2,1)S(1)} all-to-all(bf16[8,8,128]{2,1,0:T(8,128)(2,1)S(1)} %shard_map.149), channel_id=1, replica_groups=mesh['z'=8,'y'=8,'tp'=8] {'tp'}, dimensions={0} | all-to-all | bytes 32768 | tf_op jit(solution)/shard_map/all_to_all | solution.py:42
  77.9 0.0 copy-done.4
  77.9 0.0 copy-done.6
  77.9 0.0 copy-done
  77.9 0.0 copy-done.1
  77.9 0.3 shard_map.150
  78.3 15.3 %all_to_all.45.got = bf16[64,8,128]{2,1,0:T(8,128)(2,1)S(1)} all-to-all(bf16[64,8,128]{2,1,0:T(8,128)(2,1)S(1)} %bitcast.11), channel_id=1, replica_groups=mesh['z'=8,'y'=8,'tp'=8] {'z','y'}, dimensions={0} | all-to-all | bytes 262144 | tf_op jit(solution)/shard_map/all_to_all | solution.py:42
  93.6 0.1 shard_map.151
  93.7 15.7 %all_to_all.46 = bf16[64,8,128]{2,1,0:T(8,128)(2,1)S(1)} all-to-all(bf16[64,8,128]{2,1,0:T(8,128)(2,1)S(1)} %shard_map.151), channel_id=1, replica_groups=mesh['z'=8,'y'=8,'tp'=8] {'z','y'}, dimensions={0} | all-to-all | bytes 262144 | tf_op jit(solution)/shard_map/all_to_all | solution.py:42
  109.4 0.0 copy-done.2
  109.4 0.3 shard_map.152
  109.7 9.8 %all_to_all.47.got = bf16[8,8,128]{2,1,0:T(8,128)(2,1)S(1)} all-to-all(bf16[8,8,128]{2,1,0:T(8,128)(2,1)S(1)} %shard_map.152), channel_id=1, replica_groups=mesh['z'=8,'y'=8,'tp'=8] {'tp'}, dimensions={0} | all-to-all | bytes 32768 | tf_op jit(solution)/shard_map/all_to_all | solution.py:42
  119.5 0.7 shard_map.153
  (1 shorter events, 0.0 us)
Async XLA Ops:
  37.5 25.3 %copy-start.3 = (bf16[512,64]{0,1:T(8,128)(2,1)S(1)}, bf16[512,64]{0,1:T(8,128)(2,1)}, u32[]{:S(2)}) copy-start(bf16[512,64]{0,1:T(8,128)(2,1)} %param.25) | copy-start | bytes 196612
  37.5 25.3 %copy-start.5 = (f32[128]{0:T(128)S(1)}, f32[128]{0:T(128)}, u32[]{:S(2)}) copy-start(f32[128]{0:T(128)} %param.24) | copy-start | bytes 1540
  37.5 40.4 %copy-start.4 = (bf16[16,64]{1,0:T(8,128)(2,1)S(1)}, bf16[16,64]{1,0:T(8,128)(2,1)}, u32[]{:S(2)}) copy-start(bf16[16,64]{1,0:T(8,128)(2,1)} %tokens.3) | copy-start | bytes 6148
  37.5 40.4 %copy-start.6 = (f32[64]{0:T(128)S(1)}, f32[64]{0:T(128)}, u32[]{:S(2)}) copy-start(f32[64]{0:T(128)} %param.26) | copy-start | bytes 772
  38.5 39.4 %copy-start = (bf16[64,1408]{1,0:T(8,128)(2,1)S(1)}, bf16[64,1408]{1,0:T(8,128)(2,1)}, u32[]{:S(2)}) copy-start(bf16[64,1408]{1,0:T(8,128)(2,1)} %w_gate.1) | copy-start | bytes 540676
  38.6 39.4 %copy-start.1 = (bf16[64,1408]{1,0:T(8,128)(2,1)S(1)}, bf16[64,1408]{1,0:T(8,128)(2,1)}, u32[]{:S(2)}) copy-start(bf16[64,1408]{1,0:T(8,128)(2,1)} %w_up.1) | copy-start | bytes 540676
  38.6 70.8 %copy-start.2 = (bf16[1408,64]{0,1:T(8,128)(2,1)S(1)}, bf16[1408,64]{0,1:T(8,128)(2,1)}, u32[]{:S(2)}) copy-start(bf16[1408,64]{0,1:T(8,128)(2,1)} %param.29) | copy-start | bytes 540676

commit v3 on v2

--- a/solution.py
+++ b/solution.py
@@ -237,37 +237,33 @@
     residual_out[...] = residual
     x = residual.astype(F32)
     scaled = (x * gain[...]).astype(BF)
-    gate = dot(scaled, w_gate[...])
-    up = dot(scaled, w_up[...])
     squares = jnp.broadcast_to(jnp.sum(x * x, axis=1, keepdims=True), (16, 128))
-    zeros = jnp.zeros((16, 128), F32)
-    for tile in range(12):
-        group, j = tile // 3, tile % 3
-        lanes = slice(128 * tile, 128 * tile + 128)
-        rows[pl.ds(8 * group + j, 16, stride=32), :] = gate[:, lanes] if tile < 11 else zeros
-        rows[pl.ds(8 * group + 3 + j, 16, stride=32), :] = up[:, lanes] if tile < 11 else zeros
-    for group in range(4):
-        rows[pl.ds(8 * group + 6, 16, stride=32), :] = squares
-        rows[pl.ds(8 * group + 7, 16, stride=32), :] = squares
+    for first, product in ((0, dot(scaled, w_gate[...])), (24, dot(scaled, w_up[...]))):
+        for t in range(12):
+            tile = product[:, 128 * t : 128 * t + 128] if t < 11 else squares
+            rows[pl.ds(first + 2 * t, 8, stride=48), :] = tile[0:8]
+            rows[pl.ds(first + 2 * t + 1, 8, stride=48), :] = tile[8:16]
     out[...] = rows[...].astype(BF)
 
 
 def activate(got, out):
     total = summed(got)
-    inverse = lax.rsqrt(total[6:7] / 4096 + EPS)
-    gate = inverse * total[0:3]
-    up = inverse * total[3:6]
-    hidden = gate / (1.0 + jnp.exp(-gate)) * up
-    hidden = jnp.concatenate([hidden, jnp.zeros((5, 128), F32)], axis=0).astype(BF)
-    for i in range(64):
+    squares = jnp.where((iota((24, 128), 0) & 1) == 0, total[22:23], total[23:24])
+    inverse = lax.rsqrt(squares / 4096 + EPS)
+    gate = inverse * total[0:24]
+    up = inverse * total[24:48]
+    hidden = (gate / (1.0 + jnp.exp(-gate)) * up).astype(BF)
+    for i in range(8):
         out[i] = hidden
 
 
 def narrow(got, w_down, out, rows):
     rows[...] = got[...].astype(F32)
-    hidden = jnp.concatenate(
-        [rows[pl.ds(8 * (t // 3) + t % 3, 16, stride=32), :] for t in range(11)], axis=1
-    ).astype(BF)
+    halves = [
+        jnp.concatenate([rows[pl.ds(2 * t + i, 8, stride=24), :] for t in range(11)], axis=1)
+        for i in range(2)
+    ]
+    hidden = jnp.concatenate(halves, axis=0).astype(BF)
     term = folded(dot_t(hidden, w_down[...]))
     for i in range(8):
         out[i] = term
@@ -295,7 +291,6 @@
     w_down,
 ):
     tile = pltpu.VMEM((128, 128), F32)
-    wide = pltpu.VMEM((512, 128), F32)
     sent, keys, values, limit, owner, share = run(
         project,
         (
@@ -345,13 +340,17 @@
     )
     sent, residual = run(
         widen,
-        (shape(512, 128), shape(16, 64)),
+        (shape(384, 128), shape(16, 64)),
         (exchange(sent, "tp"), tokens, mixer_gain[None], w_gate, w_up),
-        scratch=[wide],
-    )
-    sent = run(activate, shape(64, 8, 128), (exchange(sent.reshape(64, 8, 128), KV),))
+        scratch=[pltpu.VMEM((384, 128), F32)],
+    )
+    sent = run(relay, shape(8, 48, 128), (exchange(sent.reshape(8, 48, 128), "y"),))
+    sent = run(activate, shape(8, 24, 128), (exchange(sent, "z"),))
     sent = run(
-        narrow, shape(8, 8, 128), (exchange(sent, KV).reshape(512, 128), w_down.T), scratch=[wide]
+        narrow,
+        shape(8, 8, 128),
+        (exchange(sent, "y").reshape(192, 128), w_down.T),
+        scratch=[pltpu.VMEM((192, 128), F32)],
     )
     return run(finish, jax.ShapeDtypeStruct((16, 64), BF), (exchange(sent, "tp"), residual))
 

time: 121 us -> 120 us (level)
    all_to_all x8 -> x9, blocking collectives: 115 us -> 114 us  [exchange(): return lax.all_to_all(array, axis, 0, 0, tiled=True)]
    pallas_call x9 -> x10, Pallas kernels: 5.42 us -> 5.29 us  [run(): pl.pallas_call(kernel, out_shape=outs, in_specs=specs, out_specs=VMEM if...]
where the time goes in v3:
time: 120 us
  blocking collectives  114 us (95%)
  Pallas kernels  5.29 us (4%)
    all_to_all x9, blocking collectives, exchange(): return lax.all_to_all(array, axis, 0, 0, tiled=True)  114 us
    pallas_call x10, Pallas kernels, run(): pl.pallas_call(kernel, out_shape=outs, in_specs=specs, out_specs=VMEM if...  5.29 us

profile of v3, /device:TPU:1, one launch (start us, length us, event | category | flops | bytes accessed | tf_op | source)
XLA Modules:
  0.0 119.7 jit_solution(9368426775445761095)
XLA Ops:
  0.0 2.4 %shard_map.145 = (bf16[8,16,768]{2,1,0:T(8,128)(2,1)S(1)}, bf16[16,512,128]{2,1,0:T(8,128)(2,1)S(1)}, bf16[16,512,128]{2,1,0:T(8,128)(2,1)S(1)}, s32[128,128]{1,...) custom-call(bf16[16,64]{1,0:T(8,128)(2,1)} %tokens.3, f32[1,64]{1,0:T(1,128)} %bitcast.17, ...), custom_call_target="tpu_custom_call" | custom-call | tf_op jit(solution)/shard_map/pallas_call | solution.py:26
  2.5 16.2 %all_to_all.45.got = bf16[8,16,768]{2,1,0:T(8,128)(2,1)S(1)} all-to-all(bf16[8,16,768]{2,1,0:T(8,128)(2,1)S(1)} %get-tuple-element.13), channel_id=1, replica_groups=mesh['z'=8,'y'=8,'tp'=8] {'y'}, dimensions={0} | all-to-all | bytes 393216 | tf_op jit(solution)/shard_map/all_to_all | solution.py:42
  18.7 18.8 %all_to_all.46.got = bf16[8,16,768]{2,1,0:T(8,128)(2,1)S(1)} all-to-all(bf16[8,16,768]{2,1,0:T(8,128)(2,1)S(1)} %shard_map.146), channel_id=1, replica_groups=mesh['z'=8,'y'=8,'tp'=8] {'z'}, dimensions={0} | all-to-all | bytes 393216 | tf_op jit(solution)/shard_map/all_to_all | solution.py:42
  37.5 0.0 copy-start.3
  37.5 0.0 copy-start.5
  37.5 0.0 copy-start.4
  37.5 0.0 copy-start.6
  37.5 1.0 shard_map.147
  38.5 0.0 copy-start
  38.6 0.0 copy-start.1
  38.6 0.0 copy-start.2
  38.6 12.1 %all_to_all.47.got = bf16[8,136,128]{2,1,0:T(8,128)(2,1)S(1)} all-to-all(bf16[8,136,128]{2,1,0:T(8,128)(2,1)S(1)} %shard_map.147), channel_id=1, replica_groups=mesh['z'=8,'y'=8,'tp'=8] {'y'}, dimensions={0} | all-to-all | bytes 557056 | tf_op jit(solution)/shard_map/all_to_all | solution.py:42
  50.7 0.1 shard_map.148
  50.8 11.9 %all_to_all.48.got = bf16[8,136,128]{2,1,0:T(8,128)(2,1)S(1)} all-to-all(bf16[8,136,128]{2,1,0:T(8,128)(2,1)S(1)} %shard_map.148), channel_id=1, replica_groups=mesh['z'=8,'y'=8,'tp'=8] {'z'}, dimensions={0} | all-to-all | bytes 557056 | tf_op jit(solution)/shard_map/all_to_all | solution.py:42
  62.8 0.0 copy-done.3
  62.8 0.0 copy-done.5
  62.8 0.5 shard_map.149
  63.2 14.7 %all_to_all.49.got = bf16[8,8,128]{2,1,0:T(8,128)(2,1)S(1)} all-to-all(bf16[8,8,128]{2,1,0:T(8,128)(2,1)S(1)} %shard_map.149), channel_id=1, replica_groups=mesh['z'=8,'y'=8,'tp'=8] {'tp'}, dimensions={0} | all-to-all | bytes 32768 | tf_op jit(solution)/shard_map/all_to_all | solution.py:42
  77.9 0.0 copy-done.4
  77.9 0.0 copy-done.6
  77.9 0.0 copy-done
  77.9 0.0 copy-done.1
  77.9 0.3 shard_map.150
  78.2 9.8 %all_to_all.50.got = bf16[8,48,128]{2,1,0:T(8,128)(2,1)S(1)} all-to-all(bf16[8,48,128]{2,1,0:T(8,128)(2,1)S(1)} %bitcast.11), channel_id=1, replica_groups=mesh['z'=8,'y'=8,'tp'=8] {'y'}, dimensions={0} | all-to-all | bytes 196608 | tf_op jit(solution)/shard_map/all_to_all | solution.py:42
  88.0 10.1 %all_to_all.51.got = bf16[8,48,128]{2,1,0:T(8,128)(2,1)S(1)} all-to-all(bf16[8,48,128]{2,1,0:T(8,128)(2,1)S(1)} %shard_map.151), channel_id=1, replica_groups=mesh['z'=8,'y'=8,'tp'=8] {'z'}, dimensions={0} | all-to-all | bytes 196608 | tf_op jit(solution)/shard_map/all_to_all | solution.py:42
  98.1 9.4 %all_to_all.52 = bf16[8,24,128]{2,1,0:T(8,128)(2,1)S(1)} all-to-all(bf16[8,24,128]{2,1,0:T(8,128)(2,1)S(1)} %shard_map.152), channel_id=1, replica_groups=mesh['z'=8,'y'=8,'tp'=8] {'y'}, dimensions={0} | all-to-all | bytes 98304 | tf_op jit(solution)/shard_map/all_to_all | solution.py:42
  107.6 0.0 copy-done.2
  107.6 0.2 shard_map.153
  107.8 11.2 %all_to_all.53.got = bf16[8,8,128]{2,1,0:T(8,128)(2,1)S(1)} all-to-all(bf16[8,8,128]{2,1,0:T(8,128)(2,1)S(1)} %shard_map.153), channel_id=1, replica_groups=mesh['z'=8,'y'=8,'tp'=8] {'tp'}, dimensions={0} | all-to-all | bytes 32768 | tf_op jit(solution)/shard_map/all_to_all | solution.py:42
  119.0 0.7 shard_map.154
  (3 shorter events, 0.1 us)
Async XLA Ops:
  37.5 25.3 %copy-start.3 = (bf16[512,64]{0,1:T(8,128)(2,1)S(1)}, bf16[512,64]{0,1:T(8,128)(2,1)}, u32[]{:S(2)}) copy-start(bf16[512,64]{0,1:T(8,128)(2,1)} %param.25) | copy-start | bytes 196612
  37.5 25.3 %copy-start.5 = (f32[128]{0:T(128)S(1)}, f32[128]{0:T(128)}, u32[]{:S(2)}) copy-start(f32[128]{0:T(128)} %param.24) | copy-start | bytes 1540
  37.5 40.4 %copy-start.4 = (bf16[16,64]{1,0:T(8,128)(2,1)S(1)}, bf16[16,64]{1,0:T(8,128)(2,1)}, u32[]{:S(2)}) copy-start(bf16[16,64]{1,0:T(8,128)(2,1)} %tokens.3) | copy-start | bytes 6148
  37.5 40.4 %copy-start.6 = (f32[64]{0:T(128)S(1)}, f32[64]{0:T(128)}, u32[]{:S(2)}) copy-start(f32[64]{0:T(128)} %param.26) | copy-start | bytes 772
  38.5 39.4 %copy-start = (bf16[64,1408]{1,0:T(8,128)(2,1)S(1)}, bf16[64,1408]{1,0:T(8,128)(2,1)}, u32[]{:S(2)}) copy-start(bf16[64,1408]{1,0:T(8,128)(2,1)} %w_gate.1) | copy-start | bytes 540676
  38.6 39.4 %copy-start.1 = (bf16[64,1408]{1,0:T(8,128)(2,1)S(1)}, bf16[64,1408]{1,0:T(8,128)(2,1)}, u32[]{:S(2)}) copy-start(bf16[64,1408]{1,0:T(8,128)(2,1)} %w_up.1) | copy-start | bytes 540676
  38.6 69.0 %copy-start.2 = (bf16[1408,64]{0,1:T(8,128)(2,1)S(1)}, bf16[1408,64]{0,1:T(8,128)(2,1)}, u32[]{:S(2)}) copy-start(bf16[1408,64]{0,1:T(8,128)(2,1)} %param.29) | copy-start | bytes 540676

commit v4 on v3

--- a/solution.py
+++ b/solution.py
@@ -73,57 +73,92 @@
     return lax.broadcasted_iota(jnp.int32, shape_, dim)
 
 
+def as_row(column):
+    here = iota((16, 128), 0) == iota((16, 128), 1)
+    return jnp.sum(jnp.where(here, column, 0.0), axis=0, keepdims=True)
+
+
+def as_column(row):
+    here = iota((16, 128), 0) == iota((16, 128), 1)
+    return jnp.sum(jnp.where(here, row, 0.0), axis=1, keepdims=True)
+
+
 def project(
     tokens, gain, w_query, w_key, w_value, lengths, weight, keys, values,
-    out, keys_out, values_out, limit, owner, share,
-    tokens_in, gain_in, query_in, key_in, value_in, lengths_in, weight_in, sems,
+    out, keys_out, values_out, limit, owner, picked, share,
+    tokens_in, gain_in, query_in, key_in, value_in, lengths_in, weight_in, sems, live_sems,
 ):
     pairs = (
+        (lengths, lengths_in),
         (tokens, tokens_in),
         (gain, gain_in),
         (w_query, query_in),
         (w_key, key_in),
         (w_value, value_in),
-        (lengths, lengths_in),
         (weight, weight_in),
-        (keys, keys_out),
-        (values, values_out),
     )
     copies = [pltpu.make_async_copy(a, b, sems.at[i]) for i, (a, b) in enumerate(pairs)]
     for copy in copies:
         copy.start()
-    for copy in copies[:5]:
+    z, y = lax.axis_index("z"), lax.axis_index("y")
+    half, head = y // 4, y % 4
+    start = (z * 8 + y) * 128
+    copies[0].wait()
+
+    def cache_copies(b):
+        return (
+            pltpu.make_async_copy(keys.at[b], keys_out.at[b], live_sems.at[0, b]),
+            pltpu.make_async_copy(values.at[b], values_out.at[b], live_sems.at[1, b]),
+        )
+
+    for b in range(16):
+
+        @pl.when(lengths_in[b] > start)
+        def _(b=b):
+            for copy in cache_copies(b):
+                copy.start()
+
+    for copy in copies[1:6]:
         copy.wait()
     x = tokens_in[...].astype(F32)
     scaled = (x * gain_in[...]).astype(BF)
     query = dot(scaled, query_in[...]).astype(BF)
     key = dot(scaled, key_in[...])
     value = dot(scaled, value_in[...])
-    squares = jnp.broadcast_to(jnp.sum(x * x, axis=1, keepdims=True), (16, 128)).astype(BF)
-    for y in range(8):
-        rows = slice(8 * (y // 4), 8 * (y // 4) + 8)
-        lanes = slice(128 * (y % 4), 128 * (y % 4) + 128)
-        out[y, :, 0:512] = query
-        out[y, :, 512:640] = jnp.concatenate([key[rows, lanes], value[rows, lanes]], axis=0).astype(BF)
-        out[y, :, 640:768] = squares
-    for copy in copies[5:7]:
-        copy.wait()
-    z, y = lax.axis_index("z"), lax.axis_index("y")
-    half, head = y // 4, y % 4
-    start = (z * 8 + y) * 128
+    squares = as_row(jnp.sum(x * x, axis=1, keepdims=True))
+    squares = jnp.broadcast_to(squares, (8, 128)).astype(BF)
+    for i in range(8):
+        rows = slice(8 * (i // 4), 8 * (i // 4) + 8)
+        lanes = slice(128 * (i % 4), 128 * (i % 4) + 128)
+        for h in range(4):
+            out[i, 16 * h : 16 * h + 16, :] = query[:, 128 * h : 128 * h + 128]
+        out[i, 64:80, :] = jnp.concatenate([key[rows, lanes], value[rows, lanes]], axis=0).astype(BF)
+        out[i, 80:88, :] = squares
+    copies[6].wait()
     row_head = iota((8, 128), 0) >> 1
     same_head = (iota((8, 128), 1) & 3) == row_head
+    mine = half * 8 + z
     for b in range(16):
         at = slice(8 * b, 8 * b + 8)
         limit[at, :] = jnp.where(same_head, lengths_in[b] - start, 0)
-        mine = jnp.logical_and(z == 0, half == b // 8)
-        owner[at, :] = jnp.where(jnp.logical_and(mine, row_head == head), 1, 0)
+        owner[at, :] = jnp.where(jnp.logical_and(mine == b, row_head == head), 1, 0)
+    picked[...] = jnp.where(iota((16, 128), 0) == mine, 1.0, 0.0)
     lane_head = (iota((8, 128), 1) >> 1) & 3
     low = jnp.where(lane_head == 0, weight_in[0], weight_in[1])
     high = jnp.where(lane_head == 2, weight_in[2], weight_in[3])
     share[...] = jnp.where(lane_head < 2, low, high)
-    for copy in copies[7:]:
-        copy.wait()
+    for b in range(16):
+        alive = lengths_in[b] > start
+
+        @pl.when(jnp.logical_not(alive))
+        def _(b=b):
+            keys_out[b] = jnp.zeros((512, 128), BF)
+            values_out[b] = jnp.zeros((512, 128), BF)
+
+        @pl.when(alive)
+        def _(b=b):
+            for copy in cache_copies(b):
+                copy.wait()
 
 
 def relay(got, out):
@@ -132,27 +167,34 @@
         out[i] = total
 
 
-def attend(got, keys, values, limit, owner, out, rows_q, rows_k, rows_v, scores, acc):
+def relay_query(got, out):
     total = summed(got)
-    inverse = lax.rsqrt(total[:, 640:768] / 4096 + EPS)
+    query = total[0:64].astype(BF)
+    row = iota((8, 128), 0)
+    for i in range(8):
+        out[i, 0:64, :] = query
+        key = total[64 + i : 65 + i]
+        value = total[72 + i : 73 + i]
+        last = jnp.where(row == 0, key, jnp.where(row == 1, value, total[80:81]))
+        out[i, 64:72, :] = last.astype(BF)
+
+
+def attend(got, keys, values, limit, owner, picked, out, rows_q, scores, acc):
+    total = summed(got)
+    inverse = lax.rsqrt(as_column(total[66:67]) / 4096 + EPS)
     first = iota((16, 128), 1) < 64
     for h in range(4):
-        query = rounded(inverse * total[:, 128 * h : 128 * h + 128])
+        query = rounded(inverse * total[16 * h : 16 * h + 16])
         rows_q[pl.ds(2 * h, 16, stride=8), :] = jnp.where(first, query, 0.0)
         rows_q[pl.ds(2 * h + 1, 16, stride=8), :] = jnp.where(first, 0.0, query)
     for b in range(16):
         at = slice(8 * b, 8 * b + 8)
         scores[at, :] = dot_t(rows_q[at, :].astype(BF), keys[b])
-    for part in range(2):
-        scale = inverse[8 * part : 8 * part + 8]
-        key_new = rounded(scale * total[0:8, 512:640])
-        value_new = rounded(scale * total[8:16, 512:640])
-        for i in range(8):
-            at = pl.ds(64 * part + i, 8, stride=8)
-            rows_k[at, :] = key_new
-            rows_v[at, :] = value_new
+    scale = jnp.sum(inverse * picked[...], axis=0, keepdims=True)
+    key_new = rounded(scale * total[64:65])
+    value_new = rounded(scale * total[65:66])
     owned = owner[...] > 0
-    own = jnp.sum(rows_q[...] * rows_k[...], axis=1, keepdims=True) * 0.125
+    own = jnp.sum(rows_q[...] * key_new, axis=1, keepdims=True) * 0.125
     own = jnp.where(owned, own, FLOOR_SCORE)
     lane = iota((128, 128), 1)
     tiles, seen = [], []
@@ -175,7 +217,7 @@
     for b in range(16):
         at = slice(8 * b, 8 * b + 8)
         acc[at, :] = dot(weights[at, :], values[b])
-    body = (acc[...] + rounded(own_weight) * rows_v[...]).T.astype(BF)
+    body = (acc[...] + rounded(own_weight) * value_new).T.astype(BF)
     totals_hi = rounded(totals)
     stat = jnp.where(
         lane == 0,
@@ -291,14 +333,15 @@
     w_down,
 ):
     tile = pltpu.VMEM((128, 128), F32)
-    sent, keys, values, limit, owner, share = run(
+    sent, keys, values, limit, owner, picked, share = run(
         project,
         (
-            shape(8, 16, 768),
+            shape(8, 88, 128),
             shape(16, 512, 128),
             shape(16, 512, 128),
             shape(128, 128, kind=jnp.int32),
             shape(128, 128, kind=jnp.int32),
+            shape(16, 128, kind=F32),
             shape(8, 128, kind=F32),
         ),
         (
@@ -321,15 +364,16 @@
             pltpu.VMEM((64, 512), BF),
             pltpu.SMEM((16,), jnp.int32),
             pltpu.SMEM((4,), F32),
-            pltpu.SemaphoreType.DMA((9,)),
+            pltpu.SemaphoreType.DMA((7,)),
+            pltpu.SemaphoreType.DMA((2, 16)),
         ],
     )
-    sent = run(relay, shape(8, 16, 768), (exchange(sent, "y"),))
+    sent = run(relay_query, shape(8, 72, 128), (exchange(sent, "y"),))
     sent = run(
         attend,
         shape(8, 136, 128),
-        (exchange(sent, "z"), keys, values, limit, owner),
-        scratch=[tile, tile, tile, pltpu.VMEM((128, 512), F32), tile],
+        (exchange(sent, "z"), keys, values, limit, owner, picked),
+        scratch=[tile, pltpu.VMEM((128, 512), F32), tile],
     )
     sent = run(merge, shape(8, 136, 128), (exchange(sent, "y"),))
     sent = run(

time: 120 us -> 119 us (level)
    all_to_all x9, blocking collectives: 114 us -> 113 us  [exchange(): return lax.all_to_all(array, axis, 0, 0, tiled=True)]
where the time goes in v4:
time: 119 us
  blocking collectives  113 us (95%)
  Pallas kernels  6.1 us (5%)
    all_to_all x9, blocking collectives, exchange(): return lax.all_to_all(array, axis, 0, 0, tiled=True)  113 us
    pallas_call x10, Pallas kernels, run(): pl.pallas_call(kernel, out_shape=outs, in_specs=specs, out_specs=VMEM if...  6.1 us

profile of v4, /device:TPU:1, one launch (start us, length us, event | category | flops | bytes accessed | tf_op | source)
XLA Modules:
  0.0 118.9 jit_solution(2812035723169672212)
XLA Ops:
  0.0 3.2 %shard_map.145 = (bf16[8,88,128]{2,1,0:T(8,128)(2,1)S(1)}, bf16[16,512,128]{2,1,0:T(8,128)(2,1)S(1)}, bf16[16,512,128]{2,1,0:T(8,128)(2,1)S(1)}, s32[128,128]{1,...) custom-call(bf16[16,64]{1,0:T(8,128)(2,1)} %tokens.3, f32[1,64]{1,0:T(1,128)} %bitcast.17, ...), custom_call_target="tpu_custom_call" | custom-call | tf_op jit(solution)/shard_map/pallas_call | solution.py:26
  3.2 15.7 %all_to_all.45.got = bf16[8,88,128]{2,1,0:T(8,128)(2,1)S(1)} all-to-all(bf16[8,88,128]{2,1,0:T(8,128)(2,1)S(1)} %get-tuple-element.14), channel_id=1, replica_groups=mesh['z'=8,'y'=8,'tp'=8] {'y'}, dimensions={0} | all-to-all | bytes 360448 | tf_op jit(solution)/shard_map/all_to_all | solution.py:42
  18.9 17.7 %all_to_all.46.got = bf16[8,72,128]{2,1,0:T(8,128)(2,1)S(1)} all-to-all(bf16[8,72,128]{2,1,0:T(8,128)(2,1)S(1)} %shard_map.146), channel_id=1, replica_groups=mesh['z'=8,'y'=8,'tp'=8] {'z'}, dimensions={0} | all-to-all | bytes 294912 | tf_op jit(solution)/shard_map/all_to_all | solution.py:42
  36.6 0.0 copy-start.3
  36.7 0.0 copy-start.5
  36.7 0.0 copy-start.4
  36.7 0.0 copy-start.6
  36.7 1.1 shard_map.147
  37.7 0.0 copy-start
  37.8 0.0 copy-start.1
  37.8 0.0 copy-start.2
  37.8 12.1 %all_to_all.47.got = bf16[8,136,128]{2,1,0:T(8,128)(2,1)S(1)} all-to-all(bf16[8,136,128]{2,1,0:T(8,128)(2,1)S(1)} %shard_map.147), channel_id=1, replica_groups=mesh['z'=8,'y'=8,'tp'=8] {'y'}, dimensions={0} | all-to-all | bytes 557056 | tf_op jit(solution)/shard_map/all_to_all | solution.py:42
  49.8 0.1 shard_map.148
  49.9 11.9 %all_to_all.48.got = bf16[8,136,128]{2,1,0:T(8,128)(2,1)S(1)} all-to-all(bf16[8,136,128]{2,1,0:T(8,128)(2,1)S(1)} %shard_map.148), channel_id=1, replica_groups=mesh['z'=8,'y'=8,'tp'=8] {'z'}, dimensions={0} | all-to-all | bytes 557056 | tf_op jit(solution)/shard_map/all_to_all | solution.py:42
  61.9 0.0 copy-done.3
  61.9 0.0 copy-done.5
  61.9 0.5 shard_map.149
  62.3 14.8 %all_to_all.49.got = bf16[8,8,128]{2,1,0:T(8,128)(2,1)S(1)} all-to-all(bf16[8,8,128]{2,1,0:T(8,128)(2,1)S(1)} %shard_map.149), channel_id=1, replica_groups=mesh['z'=8,'y'=8,'tp'=8] {'tp'}, dimensions={0} | all-to-all | bytes 32768 | tf_op jit(solution)/shard_map/all_to_all | solution.py:42
  77.1 0.0 copy-done.4
  77.1 0.0 copy-done.6
  77.1 0.0 copy-done
  77.1 0.0 copy-done.1
  77.1 0.3 shard_map.150
  77.4 9.8 %all_to_all.50.got = bf16[8,48,128]{2,1,0:T(8,128)(2,1)S(1)} all-to-all(bf16[8,48,128]{2,1,0:T(8,128)(2,1)S(1)} %bitcast.11), channel_id=1, replica_groups=mesh['z'=8,'y'=8,'tp'=8] {'y'}, dimensions={0} | all-to-all | bytes 196608 | tf_op jit(solution)/shard_map/all_to_all | solution.py:42
  87.2 10.1 %all_to_all.51.got = bf16[8,48,128]{2,1,0:T(8,128)(2,1)S(1)} all-to-all(bf16[8,48,128]{2,1,0:T(8,128)(2,1)S(1)} %shard_map.151), channel_id=1, replica_groups=mesh['z'=8,'y'=8,'tp'=8] {'z'}, dimensions={0} | all-to-all | bytes 196608 | tf_op jit(solution)/shard_map/all_to_all | solution.py:42
  97.3 9.4 %all_to_all.52 = bf16[8,24,128]{2,1,0:T(8,128)(2,1)S(1)} all-to-all(bf16[8,24,128]{2,1,0:T(8,128)(2,1)S(1)} %shard_map.152), channel_id=1, replica_groups=mesh['z'=8,'y'=8,'tp'=8] {'y'}, dimensions={0} | all-to-all | bytes 98304 | tf_op jit(solution)/shard_map/all_to_all | solution.py:42
  106.8 0.0 copy-done.2
  106.8 0.2 shard_map.153
  107.0 11.2 %all_to_all.53.got = bf16[8,8,128]{2,1,0:T(8,128)(2,1)S(1)} all-to-all(bf16[8,8,128]{2,1,0:T(8,128)(2,1)S(1)} %shard_map.153), channel_id=1, replica_groups=mesh['z'=8,'y'=8,'tp'=8] {'tp'}, dimensions={0} | all-to-all | bytes 32768 | tf_op jit(solution)/shard_map/all_to_all | solution.py:42
  118.2 0.7 shard_map.154
  (3 shorter events, 0.1 us)
Async XLA Ops:
  36.6 25.2 %copy-start.3 = (bf16[512,64]{0,1:T(8,128)(2,1)S(1)}, bf16[512,64]{0,1:T(8,128)(2,1)}, u32[]{:S(2)}) copy-start(bf16[512,64]{0,1:T(8,128)(2,1)} %param.25) | copy-start | bytes 196612
  36.7 25.2 %copy-start.5 = (f32[128]{0:T(128)S(1)}, f32[128]{0:T(128)}, u32[]{:S(2)}) copy-start(f32[128]{0:T(128)} %param.24) | copy-start | bytes 1540
  36.7 40.4 %copy-start.4 = (bf16[16,64]{1,0:T(8,128)(2,1)S(1)}, bf16[16,64]{1,0:T(8,128)(2,1)}, u32[]{:S(2)}) copy-start(bf16[16,64]{1,0:T(8,128)(2,1)} %tokens.3) | copy-start | bytes 6148
  36.7 40.4 %copy-start.6 = (f32[64]{0:T(128)S(1)}, f32[64]{0:T(128)}, u32[]{:S(2)}) copy-start(f32[64]{0:T(128)} %param.26) | copy-start | bytes 772
  37.7 39.3 %copy-start = (bf16[64,1408]{1,0:T(8,128)(2,1)S(1)}, bf16[64,1408]{1,0:T(8,128)(2,1)}, u32[]{:S(2)}) copy-start(bf16[64,1408]{1,0:T(8,128)(2,1)} %w_gate.1) | copy-start | bytes 540676
  37.8 39.3 %copy-start.1 = (bf16[64,1408]{1,0:T(8,128)(2,1)S(1)}, bf16[64,1408]{1,0:T(8,128)(2,1)}, u32[]{:S(2)}) copy-start(bf16[64,1408]{1,0:T(8,128)(2,1)} %w_up.1) | copy-start | bytes 540676
  37.8 69.0 %copy-start.2 = (bf16[1408,64]{0,1:T(8,128)(2,1)S(1)}, bf16[1408,64]{0,1:T(8,128)(2,1)}, u32[]{:S(2)}) copy-start(bf16[1408,64]{0,1:T(8,128)(2,1)} %param.29) | copy-start | bytes 540676

commit v5 on v4

--- a/solution.py
+++ b/solution.py
@@ -103,7 +103,15 @@
     z, y = lax.axis_index("z"), lax.axis_index("y")
     half, head = y // 4, y % 4
     start = (z * 8 + y) * 128
-    copies[0].wait()
+    keys_out[...] = jnp.zeros((16, 512, 128), BF)
+    values_out[...] = jnp.zeros((16, 512, 128), BF)
+    mine = half * 8 + z
+    row_head = iota((8, 128), 0) >> 1
+    same_head = (iota((8, 128), 1) & 3) == row_head
+    for b in range(16):
+        own_row = jnp.logical_and(mine == b, row_head == head)
+        owner[8 * b : 8 * b + 8, :] = jnp.where(own_row, 1, 0)
+    picked[...] = jnp.where(iota((16, 128), 0) == mine, 1.0, 0.0)
 
     def cache_copies(b):
         return (
@@ -111,6 +119,7 @@
             pltpu.make_async_copy(values.at[b], values_out.at[b], live_sems.at[1, b]),
         )
 
+    copies[0].wait()
     for b in range(16):
 
         @pl.when(lengths_in[b] > start)
@@ -135,27 +144,15 @@
         out[i, 64:80, :] = jnp.concatenate([key[rows, lanes], value[rows, lanes]], axis=0).astype(BF)
         out[i, 80:88, :] = squares
     copies[6].wait()
-    row_head = iota((8, 128), 0) >> 1
-    same_head = (iota((8, 128), 1) & 3) == row_head
-    mine = half * 8 + z
-    for b in range(16):
-        at = slice(8 * b, 8 * b + 8)
-        limit[at, :] = jnp.where(same_head, lengths_in[b] - start, 0)
-        owner[at, :] = jnp.where(jnp.logical_and(mine == b, row_head == head), 1, 0)
-    picked[...] = jnp.where(iota((16, 128), 0) == mine, 1.0, 0.0)
+    for b in range(16):
+        limit[8 * b : 8 * b + 8, :] = jnp.where(same_head, lengths_in[b] - start, 0)
     lane_head = (iota((8, 128), 1) >> 1) & 3
     low = jnp.where(lane_head == 0, weight_in[0], weight_in[1])
     high = jnp.where(lane_head == 2, weight_in[2], weight_in[3])
     share[...] = jnp.where(lane_head < 2, low, high)
     for b in range(16):
-        alive = lengths_in[b] > start
-
-        @pl.when(jnp.logical_not(alive))
-        def _(b=b):
-            keys_out[b] = jnp.zeros((512, 128), BF)
-            values_out[b] = jnp.zeros((512, 128), BF)
-
-        @pl.when(alive)
+
+        @pl.when(lengths_in[b] > start)
         def _(b=b):
             for copy in cache_copies(b):
                 copy.wait()
@@ -375,11 +372,11 @@
         (exchange(sent, "z"), keys, values, limit, owner, picked),
         scratch=[tile, pltpu.VMEM((128, 512), F32), tile],
     )
-    sent = run(merge, shape(8, 136, 128), (exchange(sent, "y"),))
+    sent = run(merge, shape(8, 136, 128), (exchange(sent, "z"),))
     sent = run(
         mix,
         shape(8, 8, 128),
-        (exchange(sent, "z"), share, head_gain[None], w_out.T),
+        (exchange(sent, "y"), share, head_gain[None], w_out.T),
         scratch=[tile],
     )
     sent, residual = run(

time: 119 us -> 119 us (level)
  no operation moved by 1% of the time
where the time goes in v5:
time: 119 us; the launch traced here: 118 us
  blocking collectives  112 us (94%)
  Pallas kernels  6.1 us (5%)
    all_to_all x9, blocking collectives, exchange(): return lax.all_to_all(array, axis, 0, 0, tiled=True)  112 us
    pallas_call x10, Pallas kernels, run(): pl.pallas_call(kernel, out_shape=outs, in_specs=specs, out_specs=VMEM if...  6.1 us

profile of v5, /device:TPU:1, one launch (start us, length us, event | category | flops | bytes accessed | tf_op | source)
XLA Modules:
  0.0 118.4 jit_solution(17686372405865312468)
XLA Ops:
  0.0 3.2 %shard_map.145 = (bf16[8,88,128]{2,1,0:T(8,128)(2,1)S(1)}, bf16[16,512,128]{2,1,0:T(8,128)(2,1)S(1)}, bf16[16,512,128]{2,1,0:T(8,128)(2,1)S(1)}, s32[128,128]{1,...) custom-call(bf16[16,64]{1,0:T(8,128)(2,1)} %tokens.3, f32[1,64]{1,0:T(1,128)} %bitcast.17, ...), custom_call_target="tpu_custom_call" | custom-call | tf_op jit(solution)/shard_map/pallas_call | solution.py:26
  3.2 15.7 %all_to_all.45.got = bf16[8,88,128]{2,1,0:T(8,128)(2,1)S(1)} all-to-all(bf16[8,88,128]{2,1,0:T(8,128)(2,1)S(1)} %get-tuple-element.14), channel_id=1, replica_groups=mesh['z'=8,'y'=8,'tp'=8] {'y'}, dimensions={0} | all-to-all | bytes 360448 | tf_op jit(solution)/shard_map/all_to_all | solution.py:42
  18.9 17.3 %all_to_all.46.got = bf16[8,72,128]{2,1,0:T(8,128)(2,1)S(1)} all-to-all(bf16[8,72,128]{2,1,0:T(8,128)(2,1)S(1)} %shard_map.146), channel_id=1, replica_groups=mesh['z'=8,'y'=8,'tp'=8] {'z'}, dimensions={0} | all-to-all | bytes 294912 | tf_op jit(solution)/shard_map/all_to_all | solution.py:42
  36.2 0.0 copy-start.3
  36.2 0.0 copy-start.5
  36.2 0.0 copy-start.4
  36.2 0.0 copy-start.6
  36.2 1.1 shard_map.147
  37.3 0.0 copy-start
  37.3 0.0 copy-start.1
  37.3 0.0 copy-start.2
  37.4 12.1 %all_to_all.47.got = bf16[8,136,128]{2,1,0:T(8,128)(2,1)S(1)} all-to-all(bf16[8,136,128]{2,1,0:T(8,128)(2,1)S(1)} %shard_map.147), channel_id=1, replica_groups=mesh['z'=8,'y'=8,'tp'=8] {'z'}, dimensions={0} | all-to-all | bytes 557056 | tf_op jit(solution)/shard_map/all_to_all | solution.py:42
  49.4 0.1 shard_map.148
  49.5 12.1 %all_to_all.48.got = bf16[8,136,128]{2,1,0:T(8,128)(2,1)S(1)} all-to-all(bf16[8,136,128]{2,1,0:T(8,128)(2,1)S(1)} %shard_map.148), channel_id=1, replica_groups=mesh['z'=8,'y'=8,'tp'=8] {'y'}, dimensions={0} | all-to-all | bytes 557056 | tf_op jit(solution)/shard_map/all_to_all | solution.py:42
  61.6 0.0 copy-done.3
  61.6 0.0 copy-done.5
  61.6 0.5 shard_map.149
  62.1 14.6 %all_to_all.49.got = bf16[8,8,128]{2,1,0:T(8,128)(2,1)S(1)} all-to-all(bf16[8,8,128]{2,1,0:T(8,128)(2,1)S(1)} %shard_map.149), channel_id=1, replica_groups=mesh['z'=8,'y'=8,'tp'=8] {'tp'}, dimensions={0} | all-to-all | bytes 32768 | tf_op jit(solution)/shard_map/all_to_all | solution.py:42
  76.7 0.0 copy-done.4
  76.7 0.0 copy-done.6
  76.7 0.0 copy-done
  76.7 0.0 copy-done.1
  76.7 0.3 shard_map.150
  77.0 9.8 %all_to_all.50.got = bf16[8,48,128]{2,1,0:T(8,128)(2,1)S(1)} all-to-all(bf16[8,48,128]{2,1,0:T(8,128)(2,1)S(1)} %bitcast.11), channel_id=1, replica_groups=mesh['z'=8,'y'=8,'tp'=8] {'y'}, dimensions={0} | all-to-all | bytes 196608 | tf_op jit(solution)/shard_map/all_to_all | solution.py:42
  86.8 10.1 %all_to_all.51.got = bf16[8,48,128]{2,1,0:T(8,128)(2,1)S(1)} all-to-all(bf16[8,48,128]{2,1,0:T(8,128)(2,1)S(1)} %shard_map.151), channel_id=1, replica_groups=mesh['z'=8,'y'=8,'tp'=8] {'z'}, dimensions={0} | all-to-all | bytes 196608 | tf_op jit(solution)/shard_map/all_to_all | solution.py:42
  96.9 9.4 %all_to_all.52 = bf16[8,24,128]{2,1,0:T(8,128)(2,1)S(1)} all-to-all(bf16[8,24,128]{2,1,0:T(8,128)(2,1)S(1)} %shard_map.152), channel_id=1, replica_groups=mesh['z'=8,'y'=8,'tp'=8] {'y'}, dimensions={0} | all-to-all | bytes 98304 | tf_op jit(solution)/shard_map/all_to_all | solution.py:42
  106.3 0.0 copy-done.2
  106.3 0.2 shard_map.153
  106.5 11.2 %all_to_all.53.got = bf16[8,8,128]{2,1,0:T(8,128)(2,1)S(1)} all-to-all(bf16[8,8,128]{2,1,0:T(8,128)(2,1)S(1)} %shard_map.153), channel_id=1, replica_groups=mesh['z'=8,'y'=8,'tp'=8] {'tp'}, dimensions={0} | all-to-all | bytes 32768 | tf_op jit(solution)/shard_map/all_to_all | solution.py:42
  117.8 0.7 shard_map.154
  (3 shorter events, 0.1 us)
Async XLA Ops:
  36.2 25.4 %copy-start.3 = (bf16[512,64]{0,1:T(8,128)(2,1)S(1)}, bf16[512,64]{0,1:T(8,128)(2,1)}, u32[]{:S(2)}) copy-start(bf16[512,64]{0,1:T(8,128)(2,1)} %param.25) | copy-start | bytes 196612
  36.2 25.4 %copy-start.5 = (f32[128]{0:T(128)S(1)}, f32[128]{0:T(128)}, u32[]{:S(2)}) copy-start(f32[128]{0:T(128)} %param.24) | copy-start | bytes 1540
  36.2 40.4 %copy-start.4 = (bf16[16,64]{1,0:T(8,128)(2,1)S(1)}, bf16[16,64]{1,0:T(8,128)(2,1)}, u32[]{:S(2)}) copy-start(bf16[16,64]{1,0:T(8,128)(2,1)} %tokens.3) | copy-start | bytes 6148
  36.2 40.4 %copy-start.6 = (f32[64]{0:T(128)S(1)}, f32[64]{0:T(128)}, u32[]{:S(2)}) copy-start(f32[64]{0:T(128)} %param.26) | copy-start | bytes 772
  37.3 39.3 %copy-start = (bf16[64,1408]{1,0:T(8,128)(2,1)S(1)}, bf16[64,1408]{1,0:T(8,128)(2,1)}, u32[]{:S(2)}) copy-start(bf16[64,1408]{1,0:T(8,128)(2,1)} %w_gate.1) | copy-start | bytes 540676
  37.3 39.3 %copy-start.1 = (bf16[64,1408]{1,0:T(8,128)(2,1)S(1)}, bf16[64,1408]{1,0:T(8,128)(2,1)}, u32[]{:S(2)}) copy-start(bf16[64,1408]{1,0:T(8,128)(2,1)} %w_up.1) | copy-start | bytes 540676
  37.3 69.0 %copy-start.2 = (bf16[1408,64]{0,1:T(8,128)(2,1)S(1)}, bf16[1408,64]{0,1:T(8,128)(2,1)}, u32[]{:S(2)}) copy-start(bf16[1408,64]{0,1:T(8,128)(2,1)} %param.29) | copy-start | bytes 540676

commit v6 on v5

--- a/solution.py
+++ b/solution.py
@@ -6,7 +6,9 @@
 from jax.sharding import Mesh
 from jax.sharding import PartitionSpec as P
 
-KV = ("z", "y")
+Z = ("z_hi", "z_lo")
+KV = ("z_hi", "z_lo", "y")
+GATHER = ("z_lo", "y")
 EPS = 1e-06
 FLOOR_SCORE = -1e30
 BF = jnp.bfloat16
@@ -100,7 +102,7 @@
     copies = [pltpu.make_async_copy(a, b, sems.at[i]) for i, (a, b) in enumerate(pairs)]
     for copy in copies:
         copy.start()
-    z, y = lax.axis_index("z"), lax.axis_index("y")
+    z, y = lax.axis_index("z_hi") * 2 + lax.axis_index("z_lo"), lax.axis_index("y")
     half, head = y // 4, y % 4
     start = (z * 8 + y) * 128
     keys_out[...] = jnp.zeros((16, 512, 128), BF)
@@ -156,12 +158,6 @@
         def _(b=b):
             for copy in cache_copies(b):
                 copy.wait()
-
-
-def relay(got, out):
-    total = summed(got).astype(BF)
-    for i in range(8):
-        out[i] = total
 
 
 def relay_query(got, out):
@@ -277,33 +273,30 @@
     x = residual.astype(F32)
     scaled = (x * gain[...]).astype(BF)
     squares = jnp.broadcast_to(jnp.sum(x * x, axis=1, keepdims=True), (16, 128))
-    for first, product in ((0, dot(scaled, w_gate[...])), (24, dot(scaled, w_up[...]))):
+    for first, product in ((0, dot(scaled, w_gate[...])), (12, dot(scaled, w_up[...]))):
         for t in range(12):
             tile = product[:, 128 * t : 128 * t + 128] if t < 11 else squares
-            rows[pl.ds(first + 2 * t, 8, stride=48), :] = tile[0:8]
-            rows[pl.ds(first + 2 * t + 1, 8, stride=48), :] = tile[8:16]
-    out[...] = rows[...].astype(BF)
+            rows[pl.ds(first + t, 16, stride=24), :] = tile
+    sent = rows[...].astype(BF)
+    for i in range(4):
+        out[384 * i : 384 * i + 384, :] = sent
 
 
 def activate(got, out):
     total = summed(got)
-    squares = jnp.where((iota((24, 128), 0) & 1) == 0, total[22:23], total[23:24])
-    inverse = lax.rsqrt(squares / 4096 + EPS)
-    gate = inverse * total[0:24]
-    up = inverse * total[24:48]
-    hidden = (gate / (1.0 + jnp.exp(-gate)) * up).astype(BF)
-    for i in range(8):
+    inverse = lax.rsqrt(total[11:12] / 4096 + EPS)
+    gate = inverse * total[0:12]
+    up = inverse * total[12:24]
+    hidden = gate / (1.0 + jnp.exp(-gate)) * up
+    hidden = jnp.concatenate([hidden, jnp.zeros((4, 128), F32)], axis=0).astype(BF)
+    for i in range(16):
         out[i] = hidden
 
 
 def narrow(got, w_down, out, rows):
     rows[...] = got[...].astype(F32)
-    halves = [
-        jnp.concatenate([rows[pl.ds(2 * t + i, 8, stride=24), :] for t in range(11)], axis=1)
-        for i in range(2)
-    ]
-    hidden = jnp.concatenate(halves, axis=0).astype(BF)
-    term = folded(dot_t(hidden, w_down[...]))
+    hidden = jnp.concatenate([rows[pl.ds(t, 16, stride=16), :] for t in range(11)], axis=1)
+    term = folded(dot_t(hidden.astype(BF), w_down[...]))
     for i in range(8):
         out[i] = term
 
@@ -369,10 +362,10 @@
     sent = run(
         attend,
         shape(8, 136, 128),
-        (exchange(sent, "z"), keys, values, limit, owner, picked),
+        (exchange(sent, Z), keys, values, limit, owner, picked),
         scratch=[tile, pltpu.VMEM((128, 512), F32), tile],
     )
-    sent = run(merge, shape(8, 136, 128), (exchange(sent, "z"),))
+    sent = run(merge, shape(8, 136, 128), (exchange(sent, Z),))
     sent = run(
         mix,
         shape(8, 8, 128),
@@ -381,23 +374,22 @@
     )
     sent, residual = run(
         widen,
-        (shape(384, 128), shape(16, 64)),
+        (shape(1536, 128), shape(16, 64)),
         (exchange(sent, "tp"), tokens, mixer_gain[None], w_gate, w_up),
         scratch=[pltpu.VMEM((384, 128), F32)],
     )
-    sent = run(relay, shape(8, 48, 128), (exchange(sent.reshape(8, 48, 128), "y"),))
-    sent = run(activate, shape(8, 24, 128), (exchange(sent, "z"),))
+    sent = run(activate, shape(16, 16, 128), (exchange(sent.reshape(64, 24, 128), KV),))
     sent = run(
         narrow,
         shape(8, 8, 128),
-        (exchange(sent, "y").reshape(192, 128), w_down.T),
-        scratch=[pltpu.VMEM((192, 128), F32)],
+        (exchange(sent, GATHER).reshape(256, 128), w_down.T),
+        scratch=[pltpu.VMEM((256, 128), F32)],
     )
     return run(finish, jax.ShapeDtypeStruct((16, 64), BF), (exchange(sent, "tp"), residual))
 
 
 def solution(mesh):
-    finer = Mesh(mesh.devices.reshape(8, 8, mesh.shape["tp"]), ("z", "y", "tp"))
+    finer = Mesh(mesh.devices.reshape(4, 2, 8, mesh.shape["tp"]), (*KV, "tp"))
     return jax.shard_map(
         local,
         mesh=finer,

time: 119 us -> 119 us (level)
    all_to_all x9 -> x8, blocking collectives: 112 us -> 113 us  [exchange(): return lax.all_to_all(array, axis, 0, 0, tiled=True)]
    pallas_call x10 -> x9, Pallas kernels: 6.1 us -> 6.17 us  [run(): pl.pallas_call(kernel, out_shape=outs, in_specs=specs, out_specs=VMEM if...]
where the time goes in v6:
time: 119 us
  blocking collectives  113 us (95%)
  Pallas kernels  6.17 us (5%)
    all_to_all x8, blocking collectives, exchange(): return lax.all_to_all(array, axis, 0, 0, tiled=True)  113 us
    pallas_call x9, Pallas kernels, run(): pl.pallas_call(kernel, out_shape=outs, in_specs=specs, out_specs=VMEM if...  6.17 us

profile of v6, /device:TPU:1, one launch (start us, length us, event | category | flops | bytes accessed | tf_op | source)
XLA Modules:
  0.0 118.9 jit_solution(8164630249412075299)
XLA Ops:
  0.0 3.2 %shard_map.145 = (bf16[8,88,128]{2,1,0:T(8,128)(2,1)S(1)}, bf16[16,512,128]{2,1,0:T(8,128)(2,1)S(1)}, bf16[16,512,128]{2,1,0:T(8,128)(2,1)S(1)}, s32[128,128]{1,...) custom-call(bf16[16,64]{1,0:T(8,128)(2,1)} %tokens.3, f32[1,64]{1,0:T(1,128)} %bitcast.17, ...), custom_call_target="tpu_custom_call" | custom-call | tf_op jit(solution)/shard_map/pallas_call | solution.py:28
  3.2 15.7 %all_to_all.40.got = bf16[8,88,128]{2,1,0:T(8,128)(2,1)S(1)} all-to-all(bf16[8,88,128]{2,1,0:T(8,128)(2,1)S(1)} %get-tuple-element.14), channel_id=1, replica_groups=mesh['z_hi'=4,'z_lo'=2,'y'=8,'tp'=8] {'y'}, dimensions={0} | all-to-all | bytes 360448 | tf_op jit(solution)/shard_map/all_to_all | solution.py:44
  18.9 17.2 %all_to_all.41.got = bf16[8,72,128]{2,1,0:T(8,128)(2,1)S(1)} all-to-all(bf16[8,72,128]{2,1,0:T(8,128)(2,1)S(1)} %shard_map.146), channel_id=1, replica_groups=mesh['z_hi'=4,'z_lo'=2,'y'=8,'tp'=8] {'z_hi','z_lo'}, dimensions={0} | all-to-all | bytes 294912 | tf_op jit(solution)/shard_map/all_to_all | solution.py:44
  36.2 0.0 copy-start.3
  36.2 0.0 copy-start.5
  36.2 0.0 copy-start.4
  36.2 0.0 copy-start.6
  36.2 1.1 shard_map.147
  37.3 0.0 copy-start
  37.3 0.0 copy-start.1
  37.3 0.0 copy-start.2
  37.3 12.1 %all_to_all.42.got = bf16[8,136,128]{2,1,0:T(8,128)(2,1)S(1)} all-to-all(bf16[8,136,128]{2,1,0:T(8,128)(2,1)S(1)} %shard_map.147), channel_id=1, replica_groups=mesh['z_hi'=4,'z_lo'=2,'y'=8,'tp'=8] {'z_hi','z_lo'}, dimensions={0} | all-to-all | bytes 557056 | tf_op jit(solution)/shard_map/all_to_all | solution.py:44
  49.4 0.1 shard_map.148
  49.5 12.1 %all_to_all.43.got = bf16[8,136,128]{2,1,0:T(8,128)(2,1)S(1)} all-to-all(bf16[8,136,128]{2,1,0:T(8,128)(2,1)S(1)} %shard_map.148), channel_id=1, replica_groups=mesh['z_hi'=4,'z_lo'=2,'y'=8,'tp'=8] {'y'}, dimensions={0} | all-to-all | bytes 557056 | tf_op jit(solution)/shard_map/all_to_all | solution.py:44
  61.6 0.0 copy-done.3
  61.6 0.0 copy-done.5
  61.6 0.5 shard_map.149
  62.0 14.6 %all_to_all.44.got = bf16[8,8,128]{2,1,0:T(8,128)(2,1)S(1)} all-to-all(bf16[8,8,128]{2,1,0:T(8,128)(2,1)S(1)} %shard_map.149), channel_id=1, replica_groups=mesh['z_hi'=4,'z_lo'=2,'y'=8,'tp'=8] {'tp'}, dimensions={0} | all-to-all | bytes 32768 | tf_op jit(solution)/shard_map/all_to_all | solution.py:44
  76.6 0.0 copy-done.4
  76.6 0.0 copy-done.6
  76.6 0.0 copy-done
  76.6 0.0 copy-done.1
  76.6 0.3 shard_map.150
  76.9 19.1 %all_to_all.45.got = bf16[64,24,128]{2,1,0:T(8,128)(2,1)S(1)} all-to-all(bf16[64,24,128]{2,1,0:T(8,128)(2,1)S(1)} %bitcast.9), channel_id=1, replica_groups=mesh['z_hi'=4,'z_lo'=2,'y'=8,'tp'=8] {'z_hi','z_lo','y'}, dimensions={0} | all-to-all | bytes 786432 | tf_op jit(solution)/shard_map/all_to_all | solution.py:44
  96.0 0.1 shard_map.151
  96.1 11.8 %all_to_all.46 = bf16[16,16,128]{2,1,0:T(8,128)(2,1)S(1)} all-to-all(bf16[16,16,128]{2,1,0:T(8,128)(2,1)S(1)} %shard_map.151), channel_id=1, replica_groups=mesh['z_hi'=4,'z_lo'=2,'y'=8,'tp'=8] {'z_lo','y'}, dimensions={0} | all-to-all | bytes 131072 | tf_op jit(solution)/shard_map/all_to_all | solution.py:44
  107.9 0.0 copy-done.2
  107.9 0.2 shard_map.152
  108.2 10.1 %all_to_all.47.got = bf16[8,8,128]{2,1,0:T(8,128)(2,1)S(1)} all-to-all(bf16[8,8,128]{2,1,0:T(8,128)(2,1)S(1)} %shard_map.152), channel_id=1, replica_groups=mesh['z_hi'=4,'z_lo'=2,'y'=8,'tp'=8] {'tp'}, dimensions={0} | all-to-all | bytes 32768 | tf_op jit(solution)/shard_map/all_to_all | solution.py:44
  118.3 0.7 shard_map.153
  (1 shorter events, 0.0 us)
Async XLA Ops:
  36.2 25.4 %copy-start.3 = (bf16[512,64]{0,1:T(8,128)(2,1)S(1)}, bf16[512,64]{0,1:T(8,128)(2,1)}, u32[]{:S(2)}) copy-start(bf16[512,64]{0,1:T(8,128)(2,1)} %param.25) | copy-start | bytes 196612
  36.2 25.4 %copy-start.5 = (f32[128]{0:T(128)S(1)}, f32[128]{0:T(128)}, u32[]{:S(2)}) copy-start(f32[128]{0:T(128)} %param.24) | copy-start | bytes 1540
  36.2 40.4 %copy-start.4 = (bf16[16,64]{1,0:T(8,128)(2,1)S(1)}, bf16[16,64]{1,0:T(8,128)(2,1)}, u32[]{:S(2)}) copy-start(bf16[16,64]{1,0:T(8,128)(2,1)} %tokens.3) | copy-start | bytes 6148
  36.2 40.4 %copy-start.6 = (f32[64]{0:T(128)S(1)}, f32[64]{0:T(128)}, u32[]{:S(2)}) copy-start(f32[64]{0:T(128)} %param.26) | copy-start | bytes 772
  37.3 39.3 %copy-start = (bf16[64,1408]{1,0:T(8,128)(2,1)S(1)}, bf16[64,1408]{1,0:T(8,128)(2,1)}, u32[]{:S(2)}) copy-start(bf16[64,1408]{1,0:T(8,128)(2,1)} %w_gate.1) | copy-start | bytes 540676
  37.3 39.3 %copy-start.1 = (bf16[64,1408]{1,0:T(8,128)(2,1)S(1)}, bf16[64,1408]{1,0:T(8,128)(2,1)}, u32[]{:S(2)}) copy-start(bf16[64,1408]{1,0:T(8,128)(2,1)} %w_up.1) | copy-start | bytes 540676
  37.3 70.6 %copy-start.2 = (bf16[1408,64]{0,1:T(8,128)(2,1)S(1)}, bf16[1408,64]{0,1:T(8,128)(2,1)}, u32[]{:S(2)}) copy-start(bf16[1408,64]{0,1:T(8,128)(2,1)} %param.29) | copy-start | bytes 540676

commit v7 on v5

--- a/solution.py
+++ b/solution.py
@@ -30,6 +30,7 @@
         out_specs=VMEM if single else [VMEM] * len(outs),
         scratch_shapes=scratch,
         compiler_params=pltpu.CompilerParams(vmem_limit_bytes=grant << 20),
+        cost_estimate=pl.CostEstimate(flops=1000000000, bytes_accessed=40000000, transcendentals=0),
         interpret=INTERPRET,
     )(*args)
 
@@ -84,17 +85,17 @@
 
 
 def project(
-    tokens, gain, w_query, w_key, w_value, lengths, weight, keys, values,
-    out, keys_out, values_out, limit, owner, picked, share,
-    tokens_in, gain_in, query_in, key_in, value_in, lengths_in, weight_in, sems, live_sems,
+    tokens, gain, w_query, w_key, w_value, lengths, weight,
+    out, limit, owner, picked, share,
+    tokens_in, gain_in, query_in, key_in, value_in, lengths_in, weight_in, sems,
 ):
     pairs = (
-        (lengths, lengths_in),
         (tokens, tokens_in),
         (gain, gain_in),
         (w_query, query_in),
         (w_key, key_in),
         (w_value, value_in),
+        (lengths, lengths_in),
         (weight, weight_in),
     )
     copies = [pltpu.make_async_copy(a, b, sems.at[i]) for i, (a, b) in enumerate(pairs)]
@@ -103,8 +104,6 @@
     z, y = lax.axis_index("z"), lax.axis_index("y")
     half, head = y // 4, y % 4
     start = (z * 8 + y) * 128
-    keys_out[...] = jnp.zeros((16, 512, 128), BF)
-    values_out[...] = jnp.zeros((16, 512, 128), BF)
     mine = half * 8 + z
     row_head = iota((8, 128), 0) >> 1
     same_head = (iota((8, 128), 1) & 3) == row_head
@@ -112,27 +111,14 @@
         own_row = jnp.logical_and(mine == b, row_head == head)
         owner[8 * b : 8 * b + 8, :] = jnp.where(own_row, 1, 0)
     picked[...] = jnp.where(iota((16, 128), 0) == mine, 1.0, 0.0)
-
-    def cache_copies(b):
-        return (
-            pltpu.make_async_copy(keys.at[b], keys_out.at[b], live_sems.at[0, b]),
-            pltpu.make_async_copy(values.at[b], values_out.at[b], live_sems.at[1, b]),
-        )
-
-    copies[0].wait()
-    for b in range(16):
-
-        @pl.when(lengths_in[b] > start)
-        def _(b=b):
-            for copy in cache_copies(b):
-                copy.start()
-
-    for copy in copies[1:6]:
+    for copy in copies[:3]:
         copy.wait()
     x = tokens_in[...].astype(F32)
     scaled = (x * gain_in[...]).astype(BF)
     query = dot(scaled, query_in[...]).astype(BF)
+    copies[3].wait()
     key = dot(scaled, key_in[...])
+    copies[4].wait()
     value = dot(scaled, value_in[...])
     squares = as_row(jnp.sum(x * x, axis=1, keepdims=True))
     squares = jnp.broadcast_to(squares, (8, 128)).astype(BF)
@@ -143,19 +129,14 @@
             out[i, 16 * h : 16 * h + 16, :] = query[:, 128 * h : 128 * h + 128]
         out[i, 64:80, :] = jnp.concatenate([key[rows, lanes], value[rows, lanes]], axis=0).astype(BF)
         out[i, 80:88, :] = squares
-    copies[6].wait()
+    for copy in copies[5:]:
+        copy.wait()
     for b in range(16):
         limit[8 * b : 8 * b + 8, :] = jnp.where(same_head, lengths_in[b] - start, 0)
     lane_head = (iota((8, 128), 1) >> 1) & 3
     low = jnp.where(lane_head == 0, weight_in[0], weight_in[1])
     high = jnp.where(lane_head == 2, weight_in[2], weight_in[3])
     share[...] = jnp.where(lane_head < 2, low, high)
-    for b in range(16):
-
-        @pl.when(lengths_in[b] > start)
-        def _(b=b):
-            for copy in cache_copies(b):
-                copy.wait()
 
 
 def relay(got, out):
@@ -330,12 +311,10 @@
     w_down,
 ):
     tile = pltpu.VMEM((128, 128), F32)
-    sent, keys, values, limit, owner, picked, share = run(
+    sent, limit, owner, picked, share = run(
         project,
         (
             shape(8, 88, 128),
-            shape(16, 512, 128),
-            shape(16, 512, 128),
             shape(128, 128, kind=jnp.int32),
             shape(128, 128, kind=jnp.int32),
             shape(16, 128, kind=F32),
@@ -349,10 +328,8 @@
             w_value,
             lengths,
             mix_weight,
-            key_cache.reshape(16, 512, 128),
-            value_cache.reshape(16, 512, 128),
         ),
-        specs=[HBM] * 9,
+        specs=[HBM] * 7,
         scratch=[
             pltpu.VMEM((16, 64), BF),
             pltpu.VMEM((1, 64), F32),
@@ -362,14 +339,20 @@
             pltpu.SMEM((16,), jnp.int32),
             pltpu.SMEM((4,), F32),
             pltpu.SemaphoreType.DMA((7,)),
-            pltpu.SemaphoreType.DMA((2, 16)),
         ],
     )
     sent = run(relay_query, shape(8, 72, 128), (exchange(sent, "y"),))
     sent = run(
         attend,
         shape(8, 136, 128),
-        (exchange(sent, "z"), keys, values, limit, owner, picked),
+        (
+            exchange(sent, "z"),
+            key_cache.reshape(16, 512, 128),
+            value_cache.reshape(16, 512, 128),
+            limit,
+            owner,
+            picked,
+        ),
         scratch=[tile, pltpu.VMEM((128, 512), F32), tile],
     )
     sent = run(merge, shape(8, 136, 128), (exchange(sent, "z"),))

time: 119 us -> 119 us (level)
  blocking collectives: 112 us -> 114 us
  Pallas kernels: 6.1 us -> 4.21 us
    pallas_call x10, Pallas kernels: 6.1 us -> 4.21 us  [run(): pl.pallas_call(kernel, out_shape=outs, in_specs=specs, out_specs=VMEM if...]
    all_to_all x9, blocking collectives: 112 us -> 114 us  [exchange(): return lax.all_to_all(array, axis, 0, 0, tiled=True)]
where the time goes in v7:
time: 119 us; the launch traced here: 118 us
  blocking collectives  114 us (96%)
  Pallas kernels  4.21 us (4%)
    all_to_all x9, blocking collectives, exchange(): return lax.all_to_all(array, axis, 0, 0, tiled=True)  114 us
    pallas_call x10, Pallas kernels, run(): pl.pallas_call(kernel, out_shape=outs, in_specs=specs, out_specs=VMEM if...  4.21 us

profile of v7, /device:TPU:1, one launch (start us, length us, event | category | flops | bytes accessed | tf_op | source)
XLA Modules:
  0.0 118.2 jit_solution(1779835098594589441)
XLA Ops:
  0.0 1.3 %shard_map.145 = (bf16[8,88,128]{2,1,0:T(8,128)(2,1)S(1)}, s32[128,128]{1,0:T(8,128)S(1)}, s32[128,128]{1,0:T(8,128)S(1)}, f32[16,128]{1,0:T(8,128)S(1)}, f32[8,128]{1,0:T(8,128)S(1)}) custom-call(bf16[16,64]{1,0:T(8,128)(2,1)} %tokens.3, f32[1,64]{1,0:T(1,128)} %bitcast.17, bf16[64,512]{1,0:T(8,128)(2,1)} %w_query.1, bf16[64,512]{1,0:T(8,128)(2,1)} %w_key.1, ...), custom_call_target="tpu_custom_call" | custom-call | flops 1000000000 | bytes 40000000 | tf_op jit(solution)/shard_map/pallas_call | solution.py:26
  1.3 0.0 copy-start
  1.4 0.0 copy-start.1
  1.4 16.3 %all_to_all.45.got = bf16[8,88,128]{2,1,0:T(8,128)(2,1)S(1)} all-to-all(bf16[8,88,128]{2,1,0:T(8,128)(2,1)S(1)} %get-tuple-element.12), channel_id=1, replica_groups=mesh['z'=8,'y'=8,'tp'=8] {'y'}, dimensions={0} | all-to-all | bytes 360448 | tf_op jit(solution)/shard_map/all_to_all | solution.py:43
  17.7 18.1 %all_to_all.46.got = bf16[8,72,128]{2,1,0:T(8,128)(2,1)S(1)} all-to-all(bf16[8,72,128]{2,1,0:T(8,128)(2,1)S(1)} %shard_map.146), channel_id=1, replica_groups=mesh['z'=8,'y'=8,'tp'=8] {'z'}, dimensions={0} | all-to-all | bytes 294912 | tf_op jit(solution)/shard_map/all_to_all | solution.py:43
  35.8 0.0 copy-done
  35.8 0.0 copy-done.1
  35.8 1.1 shard_map.147
  36.9 11.9 %all_to_all.47.got = bf16[8,136,128]{2,1,0:T(8,128)(2,1)S(1)} all-to-all(bf16[8,136,128]{2,1,0:T(8,128)(2,1)S(1)} %shard_map.147), channel_id=1, replica_groups=mesh['z'=8,'y'=8,'tp'=8] {'z'}, dimensions={0} | all-to-all | bytes 557056 | tf_op jit(solution)/shard_map/all_to_all | solution.py:43
  48.8 0.0 copy-start.5
  48.8 0.0 copy-start.7
  48.8 0.1 shard_map.148
  48.9 0.0 copy-start.2
  48.9 0.0 copy-start.3
  48.9 0.0 copy-start.6
  48.9 0.0 copy-start.8
  49.0 12.2 %all_to_all.48.got = bf16[8,136,128]{2,1,0:T(8,128)(2,1)S(1)} all-to-all(bf16[8,136,128]{2,1,0:T(8,128)(2,1)S(1)} %shard_map.148), channel_id=1, replica_groups=mesh['z'=8,'y'=8,'tp'=8] {'y'}, dimensions={0} | all-to-all | bytes 557056 | tf_op jit(solution)/shard_map/all_to_all | solution.py:43
  61.2 0.0 copy-done.5
  61.2 0.0 copy-done.7
  61.2 0.5 shard_map.149
  61.6 14.6 %all_to_all.49.got = bf16[8,8,128]{2,1,0:T(8,128)(2,1)S(1)} all-to-all(bf16[8,8,128]{2,1,0:T(8,128)(2,1)S(1)} %shard_map.149), channel_id=1, replica_groups=mesh['z'=8,'y'=8,'tp'=8] {'tp'}, dimensions={0} | all-to-all | bytes 32768 | tf_op jit(solution)/shard_map/all_to_all | solution.py:43
  76.2 0.0 copy-done.2
  76.2 0.0 copy-done.3
  76.3 0.0 copy-done.6
  76.3 0.0 copy-done.8
  76.3 0.3 shard_map.150
  76.5 9.8 %all_to_all.50.got = bf16[8,48,128]{2,1,0:T(8,128)(2,1)S(1)} all-to-all(bf16[8,48,128]{2,1,0:T(8,128)(2,1)S(1)} %bitcast.11), channel_id=1, replica_groups=mesh['z'=8,'y'=8,'tp'=8] {'y'}, dimensions={0} | all-to-all | bytes 196608 | tf_op jit(solution)/shard_map/all_to_all | solution.py:43
  86.4 0.0 copy-start.4
  86.4 10.2 %all_to_all.51.got = bf16[8,48,128]{2,1,0:T(8,128)(2,1)S(1)} all-to-all(bf16[8,48,128]{2,1,0:T(8,128)(2,1)S(1)} %shard_map.151), channel_id=1, replica_groups=mesh['z'=8,'y'=8,'tp'=8] {'z'}, dimensions={0} | all-to-all | bytes 196608 | tf_op jit(solution)/shard_map/all_to_all | solution.py:43
  96.6 9.4 %all_to_all.52 = bf16[8,24,128]{2,1,0:T(8,128)(2,1)S(1)} all-to-all(bf16[8,24,128]{2,1,0:T(8,128)(2,1)S(1)} %shard_map.152), channel_id=1, replica_groups=mesh['z'=8,'y'=8,'tp'=8] {'y'}, dimensions={0} | all-to-all | bytes 98304 | tf_op jit(solution)/shard_map/all_to_all | solution.py:43
  106.1 0.0 copy-done.4
  106.1 0.2 shard_map.153
  106.3 11.2 %all_to_all.53.got = bf16[8,8,128]{2,1,0:T(8,128)(2,1)S(1)} all-to-all(bf16[8,8,128]{2,1,0:T(8,128)(2,1)S(1)} %shard_map.153), channel_id=1, replica_groups=mesh['z'=8,'y'=8,'tp'=8] {'tp'}, dimensions={0} | all-to-all | bytes 32768 | tf_op jit(solution)/shard_map/all_to_all | solution.py:43
  117.5 0.7 shard_map.154
  (3 shorter events, 0.1 us)
Async XLA Ops:
  1.3 34.5 %copy-start = (bf16[16,128,4,128]{3,2,1,0:T(4,128)(2,1)S(1)}, bf16[16,128,4,128]{3,2,1,0:T(4,128)(2,1)}, u32[]{:S(2)}) copy-start(bf16[16,128,4,128]{3,2,1,0:T(4,128)(2,1)} %param.20) | copy-start | bytes 6291460
  1.4 34.4 %copy-start.1 = (bf16[16,128,4,128]{3,2,1,0:T(4,128)(2,1)S(1)}, bf16[16,128,4,128]{3,2,1,0:T(4,128)(2,1)}, u32[]{:S(2)}) copy-start(bf16[16,128,4,128]{3,2,1,0:T(4,128)(2,1)} %param.21) | copy-start | bytes 6291460
  48.8 12.4 %copy-start.5 = (bf16[512,64]{0,1:T(8,128)(2,1)S(1)}, bf16[512,64]{0,1:T(8,128)(2,1)}, u32[]{:S(2)}) copy-start(bf16[512,64]{0,1:T(8,128)(2,1)} %param.25) | copy-start | bytes 196612
  48.8 12.4 %copy-start.7 = (f32[128]{0:T(128)S(1)}, f32[128]{0:T(128)}, u32[]{:S(2)}) copy-start(f32[128]{0:T(128)} %param.24) | copy-start | bytes 1540
  48.9 27.3 %copy-start.2 = (bf16[64,1408]{1,0:T(8,128)(2,1)S(1)}, bf16[64,1408]{1,0:T(8,128)(2,1)}, u32[]{:S(2)}) copy-start(bf16[64,1408]{1,0:T(8,128)(2,1)} %w_gate.1) | copy-start | bytes 540676
  48.9 27.3 %copy-start.3 = (bf16[64,1408]{1,0:T(8,128)(2,1)S(1)}, bf16[64,1408]{1,0:T(8,128)(2,1)}, u32[]{:S(2)}) copy-start(bf16[64,1408]{1,0:T(8,128)(2,1)} %w_up.1) | copy-start | bytes 540676
  48.9 27.3 %copy-start.6 = (bf16[16,64]{1,0:T(8,128)(2,1)S(1)}, bf16[16,64]{1,0:T(8,128)(2,1)}, u32[]{:S(2)}) copy-start(bf16[16,64]{1,0:T(8,128)(2,1)} %tokens.3) | copy-start | bytes 6148
  48.9 27.3 %copy-start.8 = (f32[64]{0:T(128)S(1)}, f32[64]{0:T(128)}, u32[]{:S(2)}) copy-start(f32[64]{0:T(128)} %param.26) | copy-start | bytes 772
  86.4 19.7 %copy-start.4 = (bf16[1408,64]{0,1:T(8,128)(2,1)S(1)}, bf16[1408,64]{0,1:T(8,128)(2,1)}, u32[]{:S(2)}) copy-start(bf16[1408,64]{0,1:T(8,128)(2,1)} %param.29) | copy-start | bytes 540676

commit v8 on v7

--- a/solution.py
+++ b/solution.py
@@ -7,6 +7,21 @@
 from jax.sharding import PartitionSpec as P
 
 KV = ("z", "y")
+ALL = ("z", "y", "tp")
+
+
+def lines(along_y_on):
+    found = []
+    for t in range(8):
+        for fixed in range(8):
+            if t % 2 == along_y_on:
+                found.append([(fixed * 8 + y) * 8 + t for y in range(8)])
+            else:
+                found.append([(z * 8 + fixed) * 8 + t for z in range(8)])
+    return found
+
+
+U, W = lines(0), lines(1)
 EPS = 1e-06
 FLOOR_SCORE = -1e30
 BF = jnp.bfloat16
@@ -39,8 +54,8 @@
     return jax.ShapeDtypeStruct(dims, kind) if INTERPRET else pltpu.VMEM(dims, kind)
 
 
-def exchange(array, axis):
-    return lax.all_to_all(array, axis, 0, 0, tiled=True)
+def exchange(array, axis, groups=None):
+    return lax.all_to_all(array, axis, 0, 0, axis_index_groups=groups, tiled=True)
 
 
 def dot(left, right):
@@ -101,10 +116,11 @@
     copies = [pltpu.make_async_copy(a, b, sems.at[i]) for i, (a, b) in enumerate(pairs)]
     for copy in copies:
         copy.start()
-    z, y = lax.axis_index("z"), lax.axis_index("y")
-    half, head = y // 4, y % 4
+    z, y, even = lax.axis_index("z"), lax.axis_index("y"), lax.axis_index("tp") % 2 == 0
+    u, w = jnp.where(even, y, z), jnp.where(even, z, y)
+    half, head = u // 4, u % 4
     start = (z * 8 + y) * 128
-    mine = half * 8 + z
+    mine = half * 8 + w
     row_head = iota((8, 128), 0) >> 1
     same_head = (iota((8, 128), 1) & 3) == row_head
     for b in range(16):
@@ -341,12 +357,12 @@
             pltpu.SemaphoreType.DMA((7,)),
         ],
     )
-    sent = run(relay_query, shape(8, 72, 128), (exchange(sent, "y"),))
+    sent = run(relay_query, shape(8, 72, 128), (exchange(sent, ALL, U),))
     sent = run(
         attend,
         shape(8, 136, 128),
         (
-            exchange(sent, "z"),
+            exchange(sent, ALL, W),
             key_cache.reshape(16, 512, 128),
             value_cache.reshape(16, 512, 128),
             limit,
@@ -355,11 +371,11 @@
         ),
         scratch=[tile, pltpu.VMEM((128, 512), F32), tile],
     )
-    sent = run(merge, shape(8, 136, 128), (exchange(sent, "z"),))
+    sent = run(merge, shape(8, 136, 128), (exchange(sent, ALL, W),))
     sent = run(
         mix,
         shape(8, 8, 128),
-        (exchange(sent, "y"), share, head_gain[None], w_out.T),
+        (exchange(sent, ALL, U), share, head_gain[None], w_out.T),
         scratch=[tile],
     )
     sent, residual = run(
@@ -368,12 +384,12 @@
         (exchange(sent, "tp"), tokens, mixer_gain[None], w_gate, w_up),
         scratch=[pltpu.VMEM((384, 128), F32)],
     )
-    sent = run(relay, shape(8, 48, 128), (exchange(sent.reshape(8, 48, 128), "y"),))
-    sent = run(activate, shape(8, 24, 128), (exchange(sent, "z"),))
+    sent = run(relay, shape(8, 48, 128), (exchange(sent.reshape(8, 48, 128), ALL, U),))
+    sent = run(activate, shape(8, 24, 128), (exchange(sent, ALL, W),))
     sent = run(
         narrow,
         shape(8, 8, 128),
-        (exchange(sent, "y").reshape(192, 128), w_down.T),
+        (exchange(sent, ALL, U).reshape(192, 128), w_down.T),
         scratch=[pltpu.VMEM((192, 128), F32)],
     )
     return run(finish, jax.ShapeDtypeStruct((16, 64), BF), (exchange(sent, "tp"), residual))

time: 119 us -> 118 us (level)
  no operation moved by 1% of the time
where the time goes in v8:
time: 118 us
  blocking collectives  113 us (96%)
  Pallas kernels  4.21 us (4%)
    all_to_all x9, blocking collectives, exchange(): lax.all_to_all(array, axis, 0, 0, axis_index_groups=groups, tiled=True)  113 us
    pallas_call x10, Pallas kernels, run(): pl.pallas_call(kernel, out_shape=outs, in_specs=specs, out_specs=VMEM if...  4.21 us

profile of v8, /device:TPU:1, one launch (start us, length us, event | category | flops | bytes accessed | tf_op | source)
XLA Modules:
  0.0 117.6 jit_solution(11470277711345577793)
XLA Ops:
  0.0 1.3 %shard_map.145 = (bf16[8,88,128]{2,1,0:T(8,128)(2,1)S(1)}, s32[128,128]{1,0:T(8,128)S(1)}, s32[128,128]{1,0:T(8,128)S(1)}, f32[16,128]{1,0:T(8,128)S(1)}, f32[8,128]{1,0:T(8,128)S(1)}) custom-call(bf16[16,64]{1,0:T(8,128)(2,1)} %tokens.3, f32[1,64]{1,0:T(1,128)} %bitcast.17, bf16[64,512]{1,0:T(8,128)(2,1)} %w_query.1, bf16[64,512]{1,0:T(8,128)(2,1)} %w_key.1, ...), custom_call_target="tpu_custom_call" | custom-call | flops 1000000000 | bytes 40000000 | tf_op jit(solution)/shard_map/pallas_call | solution.py:41
  1.3 0.0 copy-start
  1.4 0.0 copy-start.1
  1.4 19.4 %all_to_all.45.got = bf16[8,88,128]{2,1,0:T(8,128)(2,1)S(1)} all-to-all(bf16[8,88,128]{2,1,0:T(8,128)(2,1)S(1)} %get-tuple-element.12), channel_id=1, replica_groups={{0,8,16,24,32,40,48,56},{64,72,80,88,96,104,112,120},{128,136,144,152,1..., dimensions={0} | all-to-all | bytes 360448 | tf_op jit(solution)/shard_map/all_to_all | solution.py:58
  20.8 14.7 %all_to_all.46.got = bf16[8,72,128]{2,1,0:T(8,128)(2,1)S(1)} all-to-all(bf16[8,72,128]{2,1,0:T(8,128)(2,1)S(1)} %shard_map.146), channel_id=1, replica_groups={{0,64,128,192,256,320,384,448},{8,72,136,200,264,328,392,456},{16,80,14..., dimensions={0} | all-to-all | bytes 294912 | tf_op jit(solution)/shard_map/all_to_all | solution.py:58
  35.5 0.0 copy-done
  35.5 0.0 copy-done.1
  35.5 1.1 shard_map.147
  36.6 11.9 %all_to_all.47.got = bf16[8,136,128]{2,1,0:T(8,128)(2,1)S(1)} all-to-all(bf16[8,136,128]{2,1,0:T(8,128)(2,1)S(1)} %shard_map.147), channel_id=1, replica_groups={{0,64,128,192,256,320,384,448},{8,72,136,200,264,328,392,456},{16,80,14..., dimensions={0} | all-to-all | bytes 557056 | tf_op jit(solution)/shard_map/all_to_all | solution.py:58
  48.5 0.0 copy-start.5
  48.5 0.0 copy-start.7
  48.5 0.1 shard_map.148
  48.6 0.0 copy-start.2
  48.6 0.0 copy-start.3
  48.6 0.0 copy-start.6
  48.6 0.0 copy-start.8
  48.7 12.0 %all_to_all.48.got = bf16[8,136,128]{2,1,0:T(8,128)(2,1)S(1)} all-to-all(bf16[8,136,128]{2,1,0:T(8,128)(2,1)S(1)} %shard_map.148), channel_id=1, replica_groups={{0,8,16,24,32,40,48,56},{64,72,80,88,96,104,112,120},{128,136,144,152,1..., dimensions={0} | all-to-all | bytes 557056 | tf_op jit(solution)/shard_map/all_to_all | solution.py:58
  60.7 0.0 copy-done.5
  60.7 0.0 copy-done.7
  60.7 0.5 shard_map.149
  61.2 14.6 %all_to_all.49.got = bf16[8,8,128]{2,1,0:T(8,128)(2,1)S(1)} all-to-all(bf16[8,8,128]{2,1,0:T(8,128)(2,1)S(1)} %shard_map.149), channel_id=1, replica_groups=mesh['z'=8,'y'=8,'tp'=8] {'tp'}, dimensions={0} | all-to-all | bytes 32768 | tf_op jit(solution)/shard_map/all_to_all | solution.py:58
  75.7 0.0 copy-done.2
  75.7 0.0 copy-done.3
  75.7 0.0 copy-done.6
  75.7 0.0 copy-done.8
  75.8 0.3 shard_map.150
  76.0 10.0 %all_to_all.50.got = bf16[8,48,128]{2,1,0:T(8,128)(2,1)S(1)} all-to-all(bf16[8,48,128]{2,1,0:T(8,128)(2,1)S(1)} %bitcast.11), channel_id=1, replica_groups={{0,8,16,24,32,40,48,56},{64,72,80,88,96,104,112,120},{128,136,144,152,1..., dimensions={0} | all-to-all | bytes 196608 | tf_op jit(solution)/shard_map/all_to_all | solution.py:58
  86.0 0.0 copy-start.4
  86.0 10.1 %all_to_all.51.got = bf16[8,48,128]{2,1,0:T(8,128)(2,1)S(1)} all-to-all(bf16[8,48,128]{2,1,0:T(8,128)(2,1)S(1)} %shard_map.151), channel_id=1, replica_groups={{0,64,128,192,256,320,384,448},{8,72,136,200,264,328,392,456},{16,80,14..., dimensions={0} | all-to-all | bytes 196608 | tf_op jit(solution)/shard_map/all_to_all | solution.py:58
  96.1 9.4 %all_to_all.52 = bf16[8,24,128]{2,1,0:T(8,128)(2,1)S(1)} all-to-all(bf16[8,24,128]{2,1,0:T(8,128)(2,1)S(1)} %shard_map.152), channel_id=1, replica_groups={{0,8,16,24,32,40,48,56},{64,72,80,88,96,104,112,120},{128,136,144,152,1..., dimensions={0} | all-to-all | bytes 98304 | tf_op jit(solution)/shard_map/all_to_all | solution.py:58
  105.6 0.0 copy-done.4
  105.6 0.2 shard_map.153
  105.8 11.2 %all_to_all.53.got = bf16[8,8,128]{2,1,0:T(8,128)(2,1)S(1)} all-to-all(bf16[8,8,128]{2,1,0:T(8,128)(2,1)S(1)} %shard_map.153), channel_id=1, replica_groups=mesh['z'=8,'y'=8,'tp'=8] {'tp'}, dimensions={0} | all-to-all | bytes 32768 | tf_op jit(solution)/shard_map/all_to_all | solution.py:58
  117.0 0.7 shard_map.154
  (3 shorter events, 0.1 us)
Async XLA Ops:
  1.3 34.2 %copy-start = (bf16[16,128,4,128]{3,2,1,0:T(4,128)(2,1)S(1)}, bf16[16,128,4,128]{3,2,1,0:T(4,128)(2,1)}, u32[]{:S(2)}) copy-start(bf16[16,128,4,128]{3,2,1,0:T(4,128)(2,1)} %param.20) | copy-start | bytes 6291460
  1.4 34.1 %copy-start.1 = (bf16[16,128,4,128]{3,2,1,0:T(4,128)(2,1)S(1)}, bf16[16,128,4,128]{3,2,1,0:T(4,128)(2,1)}, u32[]{:S(2)}) copy-start(bf16[16,128,4,128]{3,2,1,0:T(4,128)(2,1)} %param.21) | copy-start | bytes 6291460
  48.5 12.2 %copy-start.5 = (bf16[512,64]{0,1:T(8,128)(2,1)S(1)}, bf16[512,64]{0,1:T(8,128)(2,1)}, u32[]{:S(2)}) copy-start(bf16[512,64]{0,1:T(8,128)(2,1)} %param.25) | copy-start | bytes 196612
  48.5 12.2 %copy-start.7 = (f32[128]{0:T(128)S(1)}, f32[128]{0:T(128)}, u32[]{:S(2)}) copy-start(f32[128]{0:T(128)} %param.24) | copy-start | bytes 1540
  48.6 27.1 %copy-start.2 = (bf16[64,1408]{1,0:T(8,128)(2,1)S(1)}, bf16[64,1408]{1,0:T(8,128)(2,1)}, u32[]{:S(2)}) copy-start(bf16[64,1408]{1,0:T(8,128)(2,1)} %w_gate.1) | copy-start | bytes 540676
  48.6 27.1 %copy-start.3 = (bf16[64,1408]{1,0:T(8,128)(2,1)S(1)}, bf16[64,1408]{1,0:T(8,128)(2,1)}, u32[]{:S(2)}) copy-start(bf16[64,1408]{1,0:T(8,128)(2,1)} %w_up.1) | copy-start | bytes 540676
  48.6 27.1 %copy-start.6 = (bf16[16,64]{1,0:T(8,128)(2,1)S(1)}, bf16[16,64]{1,0:T(8,128)(2,1)}, u32[]{:S(2)}) copy-start(bf16[16,64]{1,0:T(8,128)(2,1)} %tokens.3) | copy-start | bytes 6148
  48.6 27.1 %copy-start.8 = (f32[64]{0:T(128)S(1)}, f32[64]{0:T(128)}, u32[]{:S(2)}) copy-start(f32[64]{0:T(128)} %param.26) | copy-start | bytes 772
  86.0 19.6 %copy-start.4 = (bf16[1408,64]{0,1:T(8,128)(2,1)S(1)}, bf16[1408,64]{0,1:T(8,128)(2,1)}, u32[]{:S(2)}) copy-start(bf16[1408,64]{0,1:T(8,128)(2,1)} %param.29) | copy-start | bytes 540676

commit v9 on v8

--- a/solution.py
+++ b/solution.py
@@ -10,14 +10,21 @@
 ALL = ("z", "y", "tp")
 
 
+ORDER = [0, 4, 1, 5, 2, 6, 3, 7]
+
+
+def spot(coordinate):
+    return 2 * (coordinate % 4) + coordinate // 4
+
+
 def lines(along_y_on):
     found = []
     for t in range(8):
         for fixed in range(8):
             if t % 2 == along_y_on:
-                found.append([(fixed * 8 + y) * 8 + t for y in range(8)])
+                found.append([(fixed * 8 + y) * 8 + t for y in ORDER])
             else:
-                found.append([(z * 8 + fixed) * 8 + t for z in range(8)])
+                found.append([(z * 8 + fixed) * 8 + t for z in ORDER])
     return found
 
 
@@ -117,7 +124,7 @@
     for copy in copies:
         copy.start()
     z, y, even = lax.axis_index("z"), lax.axis_index("y"), lax.axis_index("tp") % 2 == 0
-    u, w = jnp.where(even, y, z), jnp.where(even, z, y)
+    u, w = spot(jnp.where(even, y, z)), spot(jnp.where(even, z, y))
     half, head = u // 4, u % 4
     start = (z * 8 + y) * 128
     mine = half * 8 + w

time: 118 us -> 113 us (0.958)
  blocking collectives: 113 us -> 108 us
    all_to_all x9, blocking collectives: 113 us -> 108 us  [exchange(): lax.all_to_all(array, axis, 0, 0, axis_index_groups=groups, tiled=True)]
where the time goes in v9:
time: 113 us
  blocking collectives  108 us (96%)
  Pallas kernels  4.21 us (4%)
    all_to_all x9, blocking collectives, exchange(): lax.all_to_all(array, axis, 0, 0, axis_index_groups=groups, tiled=True)  108 us
    pallas_call x10, Pallas kernels, run(): pl.pallas_call(kernel, out_shape=outs, in_specs=specs, out_specs=VMEM if...  4.21 us

profile of v9, /device:TPU:1, one launch (start us, length us, event | category | flops | bytes accessed | tf_op | source)
XLA Modules:
  0.0 112.5 jit_solution(4176440233157475175)
XLA Ops:
  0.0 1.3 %shard_map.145 = (bf16[8,88,128]{2,1,0:T(8,128)(2,1)S(1)}, s32[128,128]{1,0:T(8,128)S(1)}, s32[128,128]{1,0:T(8,128)S(1)}, f32[16,128]{1,0:T(8,128)S(1)}, f32[8,128]{1,0:T(8,128)S(1)}) custom-call(bf16[16,64]{1,0:T(8,128)(2,1)} %tokens.3, f32[1,64]{1,0:T(1,128)} %bitcast.17, bf16[64,512]{1,0:T(8,128)(2,1)} %w_query.1, bf16[64,512]{1,0:T(8,128)(2,1)} %w_key.1, ...), custom_call_target="tpu_custom_call" | custom-call | flops 1000000000 | bytes 40000000 | tf_op jit(solution)/shard_map/pallas_call | solution.py:48
  1.3 0.0 copy-start
  1.4 0.0 copy-start.1
  1.4 17.7 %all_to_all.45.got = bf16[8,88,128]{2,1,0:T(8,128)(2,1)S(1)} all-to-all(bf16[8,88,128]{2,1,0:T(8,128)(2,1)S(1)} %get-tuple-element.12), channel_id=1, replica_groups={{0,32,8,40,16,48,24,56},{64,96,72,104,80,112,88,120},{128,160,136,168,1..., dimensions={0} | all-to-all | bytes 360448 | tf_op jit(solution)/shard_map/all_to_all | solution.py:65
  19.1 13.4 %all_to_all.46.got = bf16[8,72,128]{2,1,0:T(8,128)(2,1)S(1)} all-to-all(bf16[8,72,128]{2,1,0:T(8,128)(2,1)S(1)} %shard_map.146), channel_id=1, replica_groups={{0,256,64,320,128,384,192,448},{8,264,72,328,136,392,200,456},{16,272,8..., dimensions={0} | all-to-all | bytes 294912 | tf_op jit(solution)/shard_map/all_to_all | solution.py:65
  32.5 0.0 copy-done
  32.5 0.0 copy-done.1
  32.5 1.1 shard_map.147
  33.6 11.5 %all_to_all.47.got = bf16[8,136,128]{2,1,0:T(8,128)(2,1)S(1)} all-to-all(bf16[8,136,128]{2,1,0:T(8,128)(2,1)S(1)} %shard_map.147), channel_id=1, replica_groups={{0,256,64,320,128,384,192,448},{8,264,72,328,136,392,200,456},{16,272,8..., dimensions={0} | all-to-all | bytes 557056 | tf_op jit(solution)/shard_map/all_to_all | solution.py:65
  45.1 0.0 copy-start.5
  45.1 0.0 copy-start.7
  45.1 0.1 shard_map.148
  45.2 0.0 copy-start.2
  45.2 0.0 copy-start.3
  45.2 0.0 copy-start.6
  45.2 0.0 copy-start.8
  45.2 12.4 %all_to_all.48.got = bf16[8,136,128]{2,1,0:T(8,128)(2,1)S(1)} all-to-all(bf16[8,136,128]{2,1,0:T(8,128)(2,1)S(1)} %shard_map.148), channel_id=1, replica_groups={{0,32,8,40,16,48,24,56},{64,96,72,104,80,112,88,120},{128,160,136,168,1..., dimensions={0} | all-to-all | bytes 557056 | tf_op jit(solution)/shard_map/all_to_all | solution.py:65
  57.7 0.0 copy-done.5
  57.7 0.0 copy-done.7
  57.7 0.5 shard_map.149
  58.1 14.4 %all_to_all.49.got = bf16[8,8,128]{2,1,0:T(8,128)(2,1)S(1)} all-to-all(bf16[8,8,128]{2,1,0:T(8,128)(2,1)S(1)} %shard_map.149), channel_id=1, replica_groups=mesh['z'=8,'y'=8,'tp'=8] {'tp'}, dimensions={0} | all-to-all | bytes 32768 | tf_op jit(solution)/shard_map/all_to_all | solution.py:65
  72.6 0.0 copy-done.2
  72.6 0.0 copy-done.3
  72.6 0.0 copy-done.6
  72.6 0.0 copy-done.8
  72.6 0.3 shard_map.150
  72.9 9.0 %all_to_all.50.got = bf16[8,48,128]{2,1,0:T(8,128)(2,1)S(1)} all-to-all(bf16[8,48,128]{2,1,0:T(8,128)(2,1)S(1)} %bitcast.11), channel_id=1, replica_groups={{0,32,8,40,16,48,24,56},{64,96,72,104,80,112,88,120},{128,160,136,168,1..., dimensions={0} | all-to-all | bytes 196608 | tf_op jit(solution)/shard_map/all_to_all | solution.py:65
  81.9 0.0 copy-start.4
  81.9 9.2 %all_to_all.51.got = bf16[8,48,128]{2,1,0:T(8,128)(2,1)S(1)} all-to-all(bf16[8,48,128]{2,1,0:T(8,128)(2,1)S(1)} %shard_map.151), channel_id=1, replica_groups={{0,256,64,320,128,384,192,448},{8,264,72,328,136,392,200,456},{16,272,8..., dimensions={0} | all-to-all | bytes 196608 | tf_op jit(solution)/shard_map/all_to_all | solution.py:65
  91.2 9.2 %all_to_all.52 = bf16[8,24,128]{2,1,0:T(8,128)(2,1)S(1)} all-to-all(bf16[8,24,128]{2,1,0:T(8,128)(2,1)S(1)} %shard_map.152), channel_id=1, replica_groups={{0,32,8,40,16,48,24,56},{64,96,72,104,80,112,88,120},{128,160,136,168,1..., dimensions={0} | all-to-all | bytes 98304 | tf_op jit(solution)/shard_map/all_to_all | solution.py:65
  100.3 0.0 copy-done.4
  100.3 0.2 shard_map.153
  100.5 11.3 %all_to_all.53.got = bf16[8,8,128]{2,1,0:T(8,128)(2,1)S(1)} all-to-all(bf16[8,8,128]{2,1,0:T(8,128)(2,1)S(1)} %shard_map.153), channel_id=1, replica_groups=mesh['z'=8,'y'=8,'tp'=8] {'tp'}, dimensions={0} | all-to-all | bytes 32768 | tf_op jit(solution)/shard_map/all_to_all | solution.py:65
  111.9 0.7 shard_map.154
  (3 shorter events, 0.1 us)
Async XLA Ops:
  1.3 31.2 %copy-start = (bf16[16,128,4,128]{3,2,1,0:T(4,128)(2,1)S(1)}, bf16[16,128,4,128]{3,2,1,0:T(4,128)(2,1)}, u32[]{:S(2)}) copy-start(bf16[16,128,4,128]{3,2,1,0:T(4,128)(2,1)} %param.20) | copy-start | bytes 6291460
  1.4 31.1 %copy-start.1 = (bf16[16,128,4,128]{3,2,1,0:T(4,128)(2,1)S(1)}, bf16[16,128,4,128]{3,2,1,0:T(4,128)(2,1)}, u32[]{:S(2)}) copy-start(bf16[16,128,4,128]{3,2,1,0:T(4,128)(2,1)} %param.21) | copy-start | bytes 6291460
  45.1 12.6 %copy-start.5 = (bf16[512,64]{0,1:T(8,128)(2,1)S(1)}, bf16[512,64]{0,1:T(8,128)(2,1)}, u32[]{:S(2)}) copy-start(bf16[512,64]{0,1:T(8,128)(2,1)} %param.25) | copy-start | bytes 196612
  45.1 12.6 %copy-start.7 = (f32[128]{0:T(128)S(1)}, f32[128]{0:T(128)}, u32[]{:S(2)}) copy-start(f32[128]{0:T(128)} %param.24) | copy-start | bytes 1540
  45.2 27.4 %copy-start.2 = (bf16[64,1408]{1,0:T(8,128)(2,1)S(1)}, bf16[64,1408]{1,0:T(8,128)(2,1)}, u32[]{:S(2)}) copy-start(bf16[64,1408]{1,0:T(8,128)(2,1)} %w_gate.1) | copy-start | bytes 540676
  45.2 27.4 %copy-start.3 = (bf16[64,1408]{1,0:T(8,128)(2,1)S(1)}, bf16[64,1408]{1,0:T(8,128)(2,1)}, u32[]{:S(2)}) copy-start(bf16[64,1408]{1,0:T(8,128)(2,1)} %w_up.1) | copy-start | bytes 540676
  45.2 27.4 %copy-start.6 = (bf16[16,64]{1,0:T(8,128)(2,1)S(1)}, bf16[16,64]{1,0:T(8,128)(2,1)}, u32[]{:S(2)}) copy-start(bf16[16,64]{1,0:T(8,128)(2,1)} %tokens.3) | copy-start | bytes 6148
  45.2 27.4 %copy-start.8 = (f32[64]{0:T(128)S(1)}, f32[64]{0:T(128)}, u32[]{:S(2)}) copy-start(f32[64]{0:T(128)} %param.26) | copy-start | bytes 772
  81.9 18.4 %copy-start.4 = (bf16[1408,64]{0,1:T(8,128)(2,1)S(1)}, bf16[1408,64]{0,1:T(8,128)(2,1)}, u32[]{:S(2)}) copy-start(bf16[1408,64]{0,1:T(8,128)(2,1)} %param.29) | copy-start | bytes 540676
